TPU v7x, 32 devices: a whole 2x2x4 slice. The times are simulated.
32 devices in a mesh: grp: 2 (over y), sp: 4 (over z), fs: 2 (over x), tp: 2 (over core).
Axes of the slice: x: 2, y: 2, z: 4, core: 2. Of those that a mesh axis runs over, the one named last changes fastest.
Arguments:
- tokens: bfloat16 [4, 1024, 2048], P(('grp', 'fs'), 'sp', 'tp'), parts along dimension 0, may hold values from -6 to 6
- input_norm_gain: float32 [2048], replicated, may hold values from 0.1 to 1.9
- query_weight: bfloat16 [2048, 1024], P('sp', 'tp'), may hold values from -0.125 to 0.125
- key_weight: bfloat16 [2048, 1024], P('sp', 'tp'), may hold values from -0.125 to 0.125
- value_weight: bfloat16 [2048, 1024], P('sp', 'tp'), may hold values from -0.125 to 0.125
- decay_gate_weight: bfloat16 [2048, 8], replicated, may hold values from -0.125 to 0.125
- write_strength_weight: bfloat16 [2048, 8], replicated, may hold values from -0.125 to 0.125
- up_weight: bfloat16 [2048, 1024], P('sp', 'tp'), may hold values from -0.125 to 0.125
- gate_half_weight: bfloat16 [2048, 1024], P('sp', 'tp'), may hold values from -0.125 to 0.125
- log_decay_rate: float32 [8], replicated, may hold values from -30 to 0
- write_strength_bias: float32 [8], replicated, may hold values from -7 to 1
- decay_spike_added: float32 [4, 1024, 8], P(('grp', 'fs'), 'sp', 'tp'), parts along dimension 0, may hold values from -2 to 0
- starting_state: float32 [4, 8, 128, 128], P(('grp', 'fs'), 'tp'), parts along dimension 0, may hold values from -4 to 4
- head_norm_gain: float32 [128], replicated, may hold values from 0.1 to 1.9
- convolution_kernel: float32 [31, 1024], replicated, may hold values from -4 to 4
- channel_norm_gain: float32 [1024], replicated, may hold values from 0.1 to 1.9
- delta_output_rows: bfloat16 [1024, 2048], P('tp', 'sp'), may hold values from -0.125 to 0.125
- convolution_output_rows: bfloat16 [1024, 2048], P('tp', 'sp'), may hold values from -0.125 to 0.125
Outputs:
- mixed: bfloat16 [4, 1024, 2048], P(('grp', 'fs'), 'sp', 'tp'), parts along dimension 0
There are 2 independent parts, one for each index of `grp`. A program takes and returns all parts, laid end to end along the dimension named above; an argument that names none is the same for every part. Nothing has to cross between parts.
All inputs are finite; a program needn't handle non-finite values.
Results may differ from a plain program's by a relative error of at most 0.01.
Values may be sent and summed in bfloat16 or wider, within the bound.
A program may use at most 64 MiB of HBM per device.

v0:
```python
import functools

import jax
import jax.numpy as jnp
from jax import lax
from jax.experimental import pallas as pl
from jax.experimental.pallas import tpu as pltpu
from jax.sharding import PartitionSpec as P

HEAD = 128
EPS = 1e-06
HIGH = lax.Precision.HIGHEST


def from_behind(block, axis, distance):
    devices = range(lax.axis_size(axis))
    route = [(i - distance, i) for i in devices if i - distance in devices]
    return lax.ppermute(block, axis, route)


def rounded(values):
    return lax.optimization_barrier(values.astype(jnp.bfloat16)).astype(jnp.float32)


def mm(a, b, precision=None):
    return jnp.dot(a, b, preferred_element_type=jnp.float32, precision=precision)


def mm_nt(a, b, precision=None):
    return lax.dot_general(
        a, b, (((1,), (1,)), ((), ())), preferred_element_type=jnp.float32, precision=precision
    )


def mm_tn(a, b, precision=None):
    return lax.dot_general(
        a, b, (((0,), (0,)), ((), ())), preferred_element_type=jnp.float32, precision=precision
    )


def silu(x):
    return x * jax.nn.sigmoid(x)


def unit(x):
    return x * lax.rsqrt(jnp.sum(x * x, axis=-1, keepdims=True) + EPS)


MESH = pl.DeviceIdType.MESH


def column_peer(cols, sizes, index):
    where = {}
    for axis, size in reversed(list(zip(cols, sizes))):
        where[axis] = lax.rem(index, size)
        index = index // size
    return where


def column_index(cols, sizes):
    index = 0
    for axis, size in zip(cols, sizes):
        index = index * size + lax.axis_index(axis)
    return index


def greet(peers):
    barrier = pltpu.get_barrier_semaphore()
    for peer in peers:
        pl.semaphore_signal(barrier, inc=1, device_id=peer, device_id_type=MESH)
    pl.semaphore_wait(barrier, len(peers))


def send(src, dst, send_sem, recv_sem, peer):
    copy = pltpu.make_async_remote_copy(
        src_ref=src, dst_ref=dst, send_sem=send_sem, recv_sem=recv_sem, device_id=peer, device_id_type=MESH
    )
    copy.start()
    return copy


def gather_kernel(
    cols, sizes, ring, tok_ref, w_ref, spike_ref, state_ref, gain_ref, gates_ref,
    raw_ref, small_ref, spikes_ref, states_ref,
    tok_all, w_all, normed,
    tok_send, tok_recv, fwd_send, fwd_recv, w_send, w_recv, spk_send, spk_recv, st_send, st_recv, local_sem,
):
    rows, half = tok_ref.shape
    depth = w_ref.shape[0]
    count = 1
    for size in sizes:
        count *= size
    col = column_index(cols, sizes)
    tp = lax.axis_index("tp")
    sp = lax.axis_index("sp")
    partner = {"tp": 1 - tp}
    peers = [column_peer(cols, sizes, lax.rem(col + d, count)) for d in range(count)]
    right = {"sp": lax.rem(sp + 1, ring)}
    left = {"sp": lax.rem(sp + ring - 1, ring)}

    def place(source, side):
        return tok_all.at[
            pl.ds(pl.multiple_of(source * rows, rows), rows), pl.ds(pl.multiple_of(side * half, half), half)
        ]

    mid = depth // 2

    def shard(owner, top):
        begin = owner * depth + (0 if top else mid)
        return w_all.at[pl.ds(pl.multiple_of(begin, mid), mid), :]

    own = pltpu.make_async_copy(tok_ref, place(col, tp), local_sem.at[0])
    own.start()
    own_w = pltpu.make_async_copy(
        w_ref, w_all.at[pl.ds(pl.multiple_of(sp * depth, depth), depth), :], local_sem.at[1]
    )
    own_w.start()
    own_spike = pltpu.make_async_copy(spike_ref, spikes_ref.at[col], local_sem.at[2])
    own_spike.start()
    own_state = pltpu.make_async_copy(state_ref.at[col], states_ref.at[col], local_sem.at[3])
    own_state.start()
    greet([right, left, partner] + peers[1:])

    fwd = {0: send(tok_ref, place(col, tp), fwd_send.at[0], fwd_recv.at[0], partner)}
    w_copies = []

    def ring_step(step):
        behind = lax.rem(sp - step + ring, ring)
        ahead = lax.rem(sp + step, ring)
        top = w_ref.at[pl.ds(0, mid), :] if step == 0 else shard(behind, True)
        low = w_ref.at[pl.ds(mid, mid), :] if step == 0 else shard(ahead, False)
        w_copies.append(
            (
                send(top, shard(behind, True), w_send.at[0, step], w_recv.at[0, step], right),
                send(low, shard(ahead, False), w_send.at[1, step], w_recv.at[1, step], left),
            )
        )

    if ring > 1:
        ring_step(0)
    toks, spikes, states = {}, {}, {}
    for d in range(1, count):
        peer = peers[d]
        spikes[d] = send(spike_ref, spikes_ref.at[col], spk_send.at[d], spk_recv.at[d], peer)
        toks[d] = send(tok_ref, place(col, tp), tok_send.at[d], tok_recv.at[d], peer)
    for d in range(1, count):
        target = lax.rem(col + d, count)
        states[d] = send(state_ref.at[target], states_ref.at[col], st_send.at[d], st_recv.at[d], peers[d])

    def normalise(source):
        span = pl.ds(pl.multiple_of(source * rows, rows), rows)
        block = tok_all[span, :].astype(jnp.float32)
        scale = lax.rsqrt(jnp.mean(block * block, axis=-1, keepdims=True) + EPS)
        normed[span, :] = (block * scale * gain_ref[...]).astype(jnp.bfloat16)

    own.wait()
    fwd[0].wait()
    normalise(col)
    for i in range(max(ring - 1, count - 1)):
        if i < ring - 1:
            for copy in w_copies[i]:
                copy.wait()
            if i + 1 < ring - 1:
                ring_step(i + 1)
        d = i + 1
        if d < count:
            toks[d].wait()
            source = lax.rem(col - d + count, count)
            fwd[d] = send(place(source, tp), place(source, tp), fwd_send.at[d], fwd_recv.at[d], partner)
            if d > 1:
                fwd[d - 1].wait()
                normalise(lax.rem(col - d + 1 + count, count))
    if count > 1:
        fwd[count - 1].wait()
        normalise(lax.rem(col + 1, count))
    own_w.wait()
    own_spike.wait()
    own_state.wait()
    for d in range(1, count):
        spikes[d].wait()
        states[d].wait()

    @pl.loop(0, count)
    def _(c):
        span = pl.ds(pl.multiple_of(c * rows, rows), rows)
        block = normed[span, :]
        raw_ref[span, :] = mm(block, w_all[...]).astype(jnp.bfloat16)
        small_ref[span, :] = mm(block, gates_ref[...])


def gather_project(cols, sizes, ring, tokens, weights, spikes, states, gain, gates):
    rows, half = tokens.shape
    depth, width = weights.shape
    count = states.shape[0]
    total = depth * ring
    dma = pltpu.SemaphoreType.DMA
    vmem = pl.BlockSpec(memory_space=pltpu.VMEM)
    anywhere = pl.BlockSpec(memory_space=pl.ANY)
    return pl.pallas_call(
        functools.partial(gather_kernel, cols, sizes, ring),
        out_shape=(
            jax.ShapeDtypeStruct((count * rows, width), jnp.bfloat16),
            jax.ShapeDtypeStruct((count * rows, gates.shape[1]), jnp.float32),
            jax.ShapeDtypeStruct((count,) + spikes.shape, jnp.float32),
            jax.ShapeDtypeStruct(states.shape, jnp.float32),
        ),
        in_specs=[anywhere, anywhere, vmem, vmem, vmem, vmem],
        out_specs=(vmem,) * 4,
        scratch_shapes=[
            pltpu.VMEM((count * rows, total), jnp.bfloat16),
            pltpu.VMEM((total, width), jnp.bfloat16),
            pltpu.VMEM((count * rows, total), jnp.bfloat16),
            dma((count,)), dma((count,)), dma((count,)), dma((count,)),
            dma((2, ring)), dma((2, ring)),
            dma((count,)), dma((count,)), dma((count,)), dma((count,)),
            dma((4,)),
        ],
        compiler_params=pltpu.CompilerParams(
            collective_id=1, has_side_effects=True, vmem_limit_bytes=48 * 1024 * 1024
        ),
        name="gather_project",
    )(tokens, weights, spikes, states, gain, gates)


def sum_kernel(cols, sizes, x_ref, o_ref, slots, send_sem, recv_sem):
    count = slots.shape[0]
    names, widths = cols + ("tp",), sizes + (2,)
    me = column_index(names, widths)
    peers = [column_peer(names, widths, lax.rem(me + d, count)) for d in range(count)]
    greet(peers[1:])
    copies = [
        send(x_ref, slots.at[d], send_sem.at[d], recv_sem.at[d], peers[d]) for d in range(1, count)
    ]
    total = x_ref[...]
    for d in range(1, count):
        copies[d - 1].wait()
        total = total + slots[d]
    o_ref[...] = total


def sum_small(cols, sizes, x):
    count = 2
    for size in sizes:
        count *= size
    return pl.pallas_call(
        functools.partial(sum_kernel, cols, sizes),
        out_shape=jax.ShapeDtypeStruct(x.shape, x.dtype),
        in_specs=[pl.BlockSpec(memory_space=pltpu.VMEM)],
        out_specs=pl.BlockSpec(memory_space=pltpu.VMEM),
        scratch_shapes=[
            pltpu.VMEM((count,) + x.shape, x.dtype),
            pltpu.SemaphoreType.DMA((count,)),
            pltpu.SemaphoreType.DMA((count,)),
        ],
        compiler_params=pltpu.CompilerParams(collective_id=2, has_side_effects=True),
        name="sum_small",
    )(x)


def project_kernel(
    cols, sizes, mix_ref, w_ref, out_ref, to_pair, from_pair, to_col, from_col,
    pair_send, pair_recv, col_send, col_recv,
):
    count, rows, half = from_col.shape
    col = column_index(cols, sizes)
    tp = lax.axis_index("tp")
    partner = {"tp": 1 - tp}
    peers = [column_peer(cols, sizes, lax.rem(col + d, count)) for d in range(count)]
    greet([partner] + peers[1:])
    order = [d for d in range(1, count)] + [0]

    def part(d, side):
        target = lax.rem(col + d, count)
        block = mix_ref[pl.ds(pl.multiple_of(target * rows, rows), rows), :]
        return mm(block, w_ref[:, pl.ds(pl.multiple_of(side * half, half), half)])

    pairs, sends = {}, {}

    def to_partner(d):
        to_pair[d] = part(d, 1 - tp).astype(jnp.bfloat16)
        pairs[d] = send(to_pair.at[d], from_pair.at[d], pair_send.at[d], pair_recv.at[d], partner)

    to_partner(order[0])
    for i, d in enumerate(order):
        if i + 1 < count:
            to_partner(order[i + 1])
        mine = part(d, tp)
        pairs[d].wait()
        mine = mine + from_pair[d].astype(jnp.float32)
        if d:
            to_col[d] = mine.astype(jnp.bfloat16)
            sends[d] = send(to_col.at[d], from_col.at[d], col_send.at[d], col_recv.at[d], peers[d])
    total = mine
    for d in range(1, count):
        sends[d].wait()
        total = total + from_col[d].astype(jnp.float32)
    out_ref[...] = total.astype(jnp.bfloat16)


def project_out(cols, sizes, rows, mixer, weights):
    count = mixer.shape[0] // rows
    half = weights.shape[1] // 2
    bf16 = jnp.bfloat16
    dma = pltpu.SemaphoreType.DMA
    return pl.pallas_call(
        functools.partial(project_kernel, cols, sizes),
        out_shape=jax.ShapeDtypeStruct((rows, half), bf16),
        in_specs=[pl.BlockSpec(memory_space=pltpu.VMEM)] * 2,
        out_specs=pl.BlockSpec(memory_space=pltpu.VMEM),
        scratch_shapes=[pltpu.VMEM((count, rows, half), bf16)] * 4 + [dma((count,))] * 4,
        compiler_params=pltpu.CompilerParams(
            collective_id=3, has_side_effects=True, vmem_limit_bytes=48 * 1024 * 1024
        ),
        name="project_out",
    )(mixer, weights)


def delta_kernel(q_ref, k_ref, v_ref, cum_col_ref, cum_row_ref, beta_ref, p_ref, u_ref, m_ref, o_ref):
    units, rows, width = q_ref.shape
    row_id = lax.broadcasted_iota(jnp.int32, (rows, rows), 0)
    col_id = lax.broadcasted_iota(jnp.int32, (rows, rows), 1)
    lower = row_id >= col_id
    strict = row_id > col_id
    eye = jnp.where(row_id == col_id, 1.0, 0.0)
    here = range(units)
    query = [unit(silu(q_ref[u].astype(jnp.float32))) * HEAD ** (-0.5) for u in here]
    keys = [unit(silu(k_ref[u].astype(jnp.float32))) for u in here]
    values = [silu(v_ref[u].astype(jnp.float32)) for u in here]
    gamma = [
        jnp.where(lower, jnp.exp(jnp.where(lower, cum_col_ref[u] - cum_row_ref[u], 0.0)), 0.0)
        for u in here
    ]
    k_beta = [keys[u] * beta_ref[u] for u in here]
    a = [jnp.where(strict, mm_nt(k_beta[u], keys[u], HIGH) * gamma[u], 0.0) for u in here]
    size = 1
    t = None
    while size < rows:
        pair = 2 * size
        off = (row_id // pair == col_id // pair) & (row_id % pair >= size) & (col_id % pair < size)
        part = [jnp.where(off, a[u], 0.0) for u in here]
        if t is None:
            t = [eye - part[u] for u in here]
        else:
            half = [mm(part[u], t[u], HIGH) for u in here]
            t = [t[u] - mm(t[u], half[u], HIGH) for u in here]
        size = pair
    for u in here:
        grow = jnp.exp(cum_col_ref[u])
        last = cum_col_ref[u][rows - 1 :, :]
        right = jnp.concatenate([values[u] * beta_ref[u], k_beta[u] * grow], axis=1)
        solved = mm(t[u], right, HIGH)
        q_k = mm_nt(query[u], keys[u]) * gamma[u]
        k_decayed = keys[u] * jnp.exp(last - cum_col_ref[u])
        inner = mm(q_k, solved)
        p_ref[u] = query[u] * grow - inner[:, width:]
        u_ref[u] = inner[:, :width]
        state = mm_tn(k_decayed, solved, HIGH)
        m_ref[u] = eye[:width, :width] * jnp.exp(last) - state[:, width:]
        o_ref[u] = state[:, :width]


def delta_terms(query, keys, values, cum, beta):
    units, rows, width = query.shape
    f32 = jnp.float32
    group = next(g for g in (4, 2, 1) if units % g == 0)

    def spec(*dims):
        return pl.BlockSpec((group,) + dims, lambda i: (i, 0, 0))

    return pl.pallas_call(
        delta_kernel,
        grid=(units // group,),
        out_shape=(
            jax.ShapeDtypeStruct((units, rows, width), f32),
            jax.ShapeDtypeStruct((units, rows, width), f32),
            jax.ShapeDtypeStruct((units, width, width), f32),
            jax.ShapeDtypeStruct((units, width, width), f32),
        ),
        in_specs=[spec(rows, width)] * 3 + [spec(rows, 1), spec(1, rows), spec(rows, 1)],
        out_specs=(spec(rows, width), spec(rows, width), spec(width, width), spec(width, width)),
        compiler_params=pltpu.CompilerParams(vmem_limit_bytes=48 * 1024 * 1024),
        cost_estimate=pl.CostEstimate(
            flops=units * rows * rows * rows * 180, bytes_accessed=units * rows * width * 16, transcendentals=0
        ),
    )(query, keys, values, cum[..., None], cum[:, None, :], beta[..., None])


def on_device(
    cols,
    tokens,
    input_norm_gain,
    query_weight,
    key_weight,
    value_weight,
    decay_gate_weight,
    write_strength_weight,
    up_weight,
    gate_half_weight,
    log_decay_rate,
    write_strength_bias,
    decay_spike_added,
    starting_state,
    head_norm_gain,
    convolution_kernel,
    channel_norm_gain,
    delta_output_rows,
    convolution_output_rows,
):
    rows = tokens.shape[1]
    count = 1
    for axis in cols:
        count *= lax.axis_size(axis)
    channels = convolution_kernel.shape[1]
    taps = convolution_kernel.shape[0]
    tp_index = lax.axis_index("tp")
    sp_index = lax.axis_index("sp")
    col = lax.axis_index(cols) if cols else 0
    heads_tp = query_weight.shape[1] // HEAD
    heads = heads_tp // count
    chan_tp = up_weight.shape[1]
    chan = chan_tp // count
    head_start = tp_index * heads_tp + col * heads
    chan_start = tp_index * chan_tp + col * chan

    def mine(weight, axis, width):
        return lax.dynamic_slice_in_dim(weight, col * width, width, axis)

    wide = heads * HEAD
    stacked = jnp.concatenate(
        [mine(w, 1, wide) for w in (query_weight, key_weight, value_weight)]
        + [mine(w, 1, chan) for w in (up_weight, gate_half_weight)],
        axis=1,
    )
    out_rows = jnp.concatenate(
        [mine(delta_output_rows, 0, wide), mine(convolution_output_rows, 0, chan)], axis=0
    )
    sizes = tuple(lax.axis_size(axis) for axis in cols)
    gate_cols = jnp.concatenate(
        [
            lax.dynamic_slice_in_dim(decay_gate_weight, head_start, heads, 1),
            lax.dynamic_slice_in_dim(write_strength_weight, head_start, heads, 1),
        ],
        axis=1,
    )
    gate_cols = jnp.pad(gate_cols, ((0, 0), (0, 128 - 2 * heads)))
    raw, small, spikes, start_state = gather_project(
        cols,
        sizes,
        lax.axis_size("sp"),
        tokens[0],
        stacked,
        decay_spike_added[0].T.reshape((-1, 128)),
        starting_state[0].reshape((count, heads * HEAD, HEAD)),
        input_norm_gain[None],
        gate_cols,
    )
    start_state = start_state.reshape((count * heads, HEAD, HEAD))
    spikes = spikes.reshape((count, heads_tp, rows))
    spikes = jnp.swapaxes(lax.dynamic_slice_in_dim(spikes, col * heads, heads, 1), 1, 2)
    small = rounded(small[:, : 2 * heads]).reshape((count, rows, 2 * heads))
    rates = jnp.exp(lax.dynamic_slice_in_dim(log_decay_rate, head_start, heads, 0))
    bias = lax.dynamic_slice_in_dim(write_strength_bias, head_start, heads, 0)
    log_decay = -rates * jax.nn.softplus(small[..., :heads]) + spikes
    beta = jax.nn.sigmoid(small[..., heads:] + bias)
    ones = jnp.tril(jnp.ones((rows, rows), jnp.float32))
    cum = jnp.einsum("ij,cjh->chi", ones, log_decay, precision=HIGH).reshape((count * heads, rows))
    beta = jnp.swapaxes(beta, 1, 2).reshape((count * heads, rows))

    def heads_of(block):
        block = block.reshape((count, rows, heads, HEAD))
        return jnp.swapaxes(block, 1, 2).reshape((count * heads, rows, HEAD))

    p_rows, u_rows, maps, offsets = delta_terms(
        heads_of(raw[:, :wide]),
        heads_of(raw[:, wide : 2 * wide]),
        heads_of(raw[:, 2 * wide : 3 * wide]),
        cum,
        beta,
    )
    up = raw[:, 3 * wide : 3 * wide + chan].astype(jnp.float32)
    gate = raw[:, 3 * wide + chan :].astype(jnp.float32)
    glu = (up * jax.nn.sigmoid(gate)).astype(jnp.bfloat16).reshape((count, rows, chan))
    rim = from_behind(glu[:, rows - (taps - 1) :], "sp", 1)
    first = sp_index == 0
    state = jnp.where(first, start_state, jnp.zeros_like(start_state))
    for _ in range(lax.axis_size("sp") - 1):
        sent = jnp.einsum("hde,hef->hdf", maps, state, precision=HIGH) + offsets
        state = jnp.where(first, start_state, from_behind(sent, "sp", 1))

    extended = jnp.concatenate([rim, glu], axis=1).astype(jnp.float32)
    taps_here = lax.dynamic_slice_in_dim(convolution_kernel, chan_start, chan, 1)
    conv = jnp.zeros((count, rows, chan), jnp.float32)
    for tap in range(taps):
        conv = conv + taps_here[tap] * extended[:, tap : tap + rows]
    sums = jnp.stack([jnp.sum(conv, axis=-1), jnp.sum(conv * conv, axis=-1)])
    sums = sum_small(cols, sizes, sums.reshape((-1, 128))).reshape(sums.shape)
    mean_c = (sums[0] / channels)[..., None]
    var_c = (sums[1] / channels)[..., None] - mean_c * mean_c
    gain = lax.dynamic_slice_in_dim(channel_norm_gain, chan_start, chan, 0)
    conv_out = jax.nn.silu((conv - mean_c) * lax.rsqrt(var_c + EPS) * gain).astype(jnp.bfloat16)

    attn = jnp.einsum("hcd,hde->hce", p_rows, state) + u_rows
    attn_out = (
        attn * lax.rsqrt(jnp.mean(attn * attn, axis=-1, keepdims=True) + EPS) * head_norm_gain
    ).astype(jnp.bfloat16)
    attn_out = jnp.swapaxes(attn_out.reshape((count, heads, rows, HEAD)), 1, 2)
    attn_out = attn_out.reshape((count * rows, wide))
    mixer = jnp.concatenate([attn_out, conv_out.reshape((count * rows, chan))], axis=1)
    gathered_out = lax.all_gather(out_rows, "sp", axis=1, tiled=True)
    return project_out(cols, sizes, rows, mixer, gathered_out)[None]


def split_axes(mesh, heads_tp, chan_tp):
    for axes in (("grp", "fs"), ("fs",), ("grp",)):
        count = 1
        for axis in axes:
            count *= mesh.shape[axis]
        if heads_tp % count == 0 and chan_tp % (count * 128) == 0:
            return axes
    return ()


def solution(mesh):
    def whole(*args):
        heads_tp = args[2].shape[1] // HEAD // mesh.shape["tp"]
        chan_tp = args[7].shape[1] // mesh.shape["tp"]
        cols = split_axes(mesh, heads_tp, chan_tp)
        return jax.shard_map(
            functools.partial(on_device, cols),
            mesh=mesh,
            in_specs=(
                P(("grp", "fs"), "sp", "tp"),
                P(),
                P("sp", "tp"),
                P("sp", "tp"),
                P("sp", "tp"),
                P(),
                P(),
                P("sp", "tp"),
                P("sp", "tp"),
                P(),
                P(),
                P(("grp", "fs"), "sp", "tp"),
                P(("grp", "fs"), "tp", None, None),
                P(),
                P(),
                P(),
                P("tp", "sp"),
                P("tp", "sp"),
            ),
            out_specs=P(("grp", "fs"), "sp", "tp"),
            check_vma=False,
        )(*args)

    return whole
```

profile of v0, /device:TPU:0, one launch (start us, length us, event | category | flops | bytes accessed | tf_op | source)
XLA Modules:
  0.0 178.6 jit_solution(16707252931000660371)
XLA Ops:
  6.5 0.7 reshape.103.spike_ref
  7.2 0.8 constant_dynamic-slice_fusion.4
  8.4 1.0 dynamic-slice_dynamic-update-slice_fusion.4
  9.4 0.9 dynamic-slice_dynamic-update-slice_fusion.3
  10.4 0.9 dynamic-slice_dynamic-update-slice_fusion.2
  11.3 0.9 dynamic-slice_dynamic-update-slice_fusion.1
  12.3 0.9 dynamic-slice_dynamic-update-slice_fusion.w_ref
  13.3 59.0 %gather_project.1 = (bf16[1024,640]{1,0:T(8,128)(2,1)S(1)}, f32[1024,128]{1,0:T(8,128)S(1)}, f32[4,8,128]{2,1,0:T(8,128)S(1)}, f32[4,128,128]{2,1,0:T(8,128)S(1)}) custom-call(bf16[256,1024]{1,0:T(8,128)(2,1)S(1)} %bitcast.92, bf16[512,640]{1,0:T(8,128)(2,1)S(1)} %dynamic-slice_dynamic-update-slice_fusion.w_ref, f32[8,128]{1,0:T(8,128)S(1)} %reshape.103.spike_ref, ...), custom_call_target="tpu_custom_call" | custom-call | tf_op jit(solution)/shard_map/gather_project/pallas_call | solution.py:199
  72.6 2.7 %collective-permute-start.3 = (bf16[4,30,128]{2,1,0:T(8,128)(2,1)S(1)}, bf16[4,30,128]{2,1,0:T(8,128)(2,1)S(1)}, u32[]{:S(2)}, u32[]{:S(2)}) collective-permute-start(bf16[4,30,128]{2,1,0:T(8,128)(2,1)S(1)} %slice.298), channel_id=1, source_target_pairs={{0,4},{4,8},{8,12},{1,5},{5,9},{9,13},{2,6},{6,10},{10,14},{3,7},{... | collective-permute-start | bytes 92168 | tf_op jit(solution)/shard_map/ppermute | solution.py:18
  75.3 0.8 fusion.56
  76.2 0.7 dynamic_slice.51
  77.2 0.6 dynamic_slice.49
  78.5 1.2 fusion.36
  80.3 0.9 copy-done.3
  81.2 17.1 %shard_map.172 = (f32[4,256,128]{2,1,0:T(8,128)S(1)}, f32[4,256,128]{2,1,0:T(8,128)S(1)}, f32[4,128,128]{2,1,0:T(8,128)S(1)}, f32[4,128,128]{2,1,0:T(8,128)S(1)}) custom-call(bf16[4,256,128]{2,1,0:T(8,128)(2,1)S(1)} %bitcast.96, bf16[4,256,128]{2,1,0:T(8,128)(2,1)S(1)} %bitcast.95, bf16[4,256,128]{2,1,0:T(8,128)(2,1)S(1)} %bitcast.94, ...), custom_call_target="tpu_custom_call" | custom-call | flops 12079595520 | bytes 2097152 | tf_op jit(solution)/shard_map/pallas_call | solution.py:370
  98.7 3.6 %collective-permute-start = (f32[4,128,128]{2,1,0:T(8,128)S(1)}, f32[4,128,128]{2,1,0:T(8,128)S(1)}, u32[]{:S(2)}, u32[]{:S(2)}) collective-permute-start(f32[4,128,128]{2,1,0:T(8,128)S(1)} %convolution_add_fusion.3), channel_id=1, source_target_pairs={{0,4},{4,8},{8,12},{1,5},{5,9},{9,13},{2,6},{6,10},{10,14},{3,7},{... | collective-permute-start | bytes 786440 | tf_op jit(solution)/shard_map/ppermute | solution.py:18
  102.3 1.0 constant_dynamic-slice_fusion.1
  103.3 0.7 pad_maximum_fusion.1
  104.1 1.2 fusion.50
  105.3 1.1 dynamic-slice_bitcast_fusion.29
  106.3 0.8 dynamic_slice.53
  107.2 2.4 %fusion.54 = (f32[4,256]{1,0:T(4,128)S(1)}, f32[4,256]{1,0:T(4,128)S(1)}, f32[4,256,128]{2,1,0:T(8,128)S(1)}) fusion(f32[4,286,128]{2,1,0:T(8,128)S(1)} %maximum_convert_fusion, f32[128]{0:T(128)S(1)} %get-tuple-element.59, f32[128]{0:T(128)S(1)} %get-tuple-element.30, f32[128]{0:T(128)S(1)} %get-tuple-element.31, f32[128]{0:T(128)S(1)} %get-tuple-element.32, ...), kind=kLoop, calls=%fused_computation.150 | loop fusion | flops 8386560 | bytes 16801280 | tf_op jit(solution)/shard_map/reduce_sum | solution.py:495
  109.6 0.6 reshape.109.x_ref
  110.2 6.0 %sum_small.1 = f32[16,128]{1,0:T(8,128)} custom-call(f32[16,128]{1,0:T(8,128)} %reshape.109.x_ref), custom_call_target="tpu_custom_call" | custom-call | tf_op jit(solution)/shard_map/sum_small/pallas_call | solution.py:245
  116.2 0.4 convolution_add_fusion.2
  116.6 2.8 %collective-permute-start.1 = (f32[4,128,128]{2,1,0:T(8,128)S(1)}, f32[4,128,128]{2,1,0:T(8,128)S(1)}, u32[]{:S(2)}, u32[]{:S(2)}) collective-permute-start(f32[4,128,128]{2,1,0:T(8,128)S(1)} %convolution_add_fusion.2), channel_id=1, source_target_pairs={{0,4},{4,8},{8,12},{1,5},{5,9},{9,13},{2,6},{6,10},{10,14},{3,7},{... | collective-permute-start | bytes 786440 | tf_op jit(solution)/shard_map/ppermute | solution.py:18
  119.5 12.0 %collective-permute-done.1 = f32[4,128,128]{2,1,0:T(8,128)S(1)} collective-permute-done((f32[4,128,128]{2,1,0:T(8,128)S(1)}, f32[4,128,128]{2,1,0:T(8,128)S(1)}, u32[]{:S(2)}, u32[]{:S(2)}) %collective-permute-start.1) | collective-permute-done | bytes 262176 | tf_op jit(solution)/shard_map/ppermute | solution.py:18
  131.9 5.0 %collective-permute-start.2 = (bf16[4,128,128]{2,1,0:T(8,128)(2,1)S(1)}, bf16[4,128,128]{2,1,0:T(8,128)(2,1)S(1)}, u32[]{:S(2)}, u32[]{:S(2)}) collective-permute-start(bf16[4,128,128]{2,1,0:T(8,128)(2,1)S(1)} %convolution_add_fusion.1), channel_id=1, source_target_pairs={{0,4},{4,8},{8,12},{1,5},{5,9},{9,13},{2,6},{6,10},{10,14},{3,7},{... | collective-permute-start | bytes 393224 | tf_op jit(solution)/shard_map/ppermute | solution.py:18
  137.3 2.4 %collective-permute-done.2 = bf16[4,128,128]{2,1,0:T(8,128)(2,1)S(1)} collective-permute-done((bf16[4,128,128]{2,1,0:T(8,128)(2,1)S(1)}, bf16[4,128,128]{2,1,0:T(8,128)(2,1)S(1)}, u32[]{:S(2)}, u32[]{:S(2)}) %collective-permute-start.2) | collective-permute-done | bytes 131104 | tf_op jit(solution)/shard_map/ppermute | solution.py:18
  140.3 1.2 copy-done
  141.5 29.4 %project_out.1 = bf16[256,1024]{1,0:T(8,128)(2,1)S(1)} custom-call(bf16[1024,256]{1,0:T(8,128)(2,1)S(1)} %pad_maximum_fusion.mix_ref, bf16[256,2048]{1,0:T(8,128)(2,1)S(1)} %copy-done), custom_call_target="tpu_custom_call" | custom-call | tf_op jit(solution)/shard_map/project_out/pallas_call | solution.py:305
  171.0 0.8 copy.45
  (52 shorter events, 3.5 us)
Async XLA Ops:
  6.5 133.8 %all-gather.2.cloned.1.call-start = ((), (), s32[]{:S(2)}) async-start(), calls=%async_computation | async-start | bytes 1310720 | tf_op jit(solution)/shard_map/all_gather | solution.py:509
  8.4 4.9 %copy-start.1 = (bf16[1,256,1024]{2,1,0:T(8,128)(2,1)S(1)}, bf16[1,256,1024]{2,1,0:T(8,128)(2,1)}, u32[]{:S(2)}) copy-start(bf16[1,256,1024]{2,1,0:T(8,128)(2,1)} %param.18) | copy-start | bytes 1572868
  8.4 4.9 %copy-start.2 = (f32[1,4,128,128]{3,2,1,0:T(8,128)S(1)}, f32[1,4,128,128]{3,2,1,0:T(8,128)}, u32[]{:S(2)}) copy-start(f32[1,4,128,128]{3,2,1,0:T(8,128)} %param.30) | copy-start | bytes 786436
  8.4 4.9 %copy-start.4 = (f32[2048]{0:T(1024)S(1)}, f32[2048]{0:T(1024)}, u32[]{:S(2)}) copy-start(f32[2048]{0:T(1024)} %param.19) | copy-start | bytes 24580
  72.5 3.7 %copy-start.5 = (bf16[1024,128]{1,0:T(8,128)(2,1)}, bf16[1024,128]{1,0:T(8,128)(2,1)S(1)}, u32[]{:S(2)}) copy-start(bf16[1024,128]{1,0:T(8,128)(2,1)S(1)} %multiply_convert_fusion.1) | copy-start | bytes 786436
  72.6 3.7 %copy-start.9 = (f32[8]{0:T(128)S(1)}, f32[8]{0:T(128)}, u32[]{:S(2)}) copy-start(f32[8]{0:T(128)} %param.28) | copy-start | bytes 100
  72.6 34.5 %collective-permute-start.3 = (bf16[4,30,128]{2,1,0:T(8,128)(2,1)S(1)}, bf16[4,30,128]{2,1,0:T(8,128)(2,1)S(1)}, u32[]{:S(2)}, u32[]{:S(2)}) collective-permute-start(bf16[4,30,128]{2,1,0:T(8,128)(2,1)S(1)} %slice.298), channel_id=1, source_target_pairs={{0,4},{4,8},{8,12},{1,5},{5,9},{9,13},{2,6},{6,10},{10,14},{3,7},{... | collective-permute-start | bytes 92168 | tf_op jit(solution)/shard_map/ppermute | solution.py:18
  76.1 1.0 copy-start.10
  80.3 1.0 copy-start.3
  98.3 8.8 %copy-start.6 = (bf16[1024,128]{1,0:T(8,128)(2,1)S(1)}, bf16[1024,128]{1,0:T(8,128)(2,1)}, u32[]{:S(2)}) copy-start(bf16[1024,128]{1,0:T(8,128)(2,1)} %copy-done.5) | copy-start | bytes 786436
  98.7 17.5 %collective-permute-start = (f32[4,128,128]{2,1,0:T(8,128)S(1)}, f32[4,128,128]{2,1,0:T(8,128)S(1)}, u32[]{:S(2)}, u32[]{:S(2)}) collective-permute-start(f32[4,128,128]{2,1,0:T(8,128)S(1)} %convolution_add_fusion.3), channel_id=1, source_target_pairs={{0,4},{4,8},{8,12},{1,5},{5,9},{9,13},{2,6},{6,10},{10,14},{3,7},{... | collective-permute-start | bytes 786440 | tf_op jit(solution)/shard_map/ppermute | solution.py:18
  116.2 3.3 %copy-start.7 = (f32[16,128]{1,0:T(8,128)S(1)}, f32[16,128]{1,0:T(8,128)}, u32[]{:S(2)}) copy-start(f32[16,128]{1,0:T(8,128)} %sum_small.1) | copy-start | bytes 24580
  116.6 14.9 %collective-permute-start.1 = (f32[4,128,128]{2,1,0:T(8,128)S(1)}, f32[4,128,128]{2,1,0:T(8,128)S(1)}, u32[]{:S(2)}, u32[]{:S(2)}) collective-permute-start(f32[4,128,128]{2,1,0:T(8,128)S(1)} %convolution_add_fusion.2), channel_id=1, source_target_pairs={{0,4},{4,8},{8,12},{1,5},{5,9},{9,13},{2,6},{6,10},{10,14},{3,7},{... | collective-permute-start | bytes 786440 | tf_op jit(solution)/shard_map/ppermute | solution.py:18
  131.9 7.7 %collective-permute-start.2 = (bf16[4,128,128]{2,1,0:T(8,128)(2,1)S(1)}, bf16[4,128,128]{2,1,0:T(8,128)(2,1)S(1)}, u32[]{:S(2)}, u32[]{:S(2)}) collective-permute-start(bf16[4,128,128]{2,1,0:T(8,128)(2,1)S(1)} %convolution_add_fusion.1), channel_id=1, source_target_pairs={{0,4},{4,8},{8,12},{1,5},{5,9},{9,13},{2,6},{6,10},{10,14},{3,7},{... | collective-permute-start | bytes 393224 | tf_op jit(solution)/shard_map/ppermute | solution.py:18
  136.9 3.1 %copy-start.8 = (f32[128]{0:T(128)S(1)}, f32[128]{0:T(128)}, u32[]{:S(2)}) copy-start(f32[128]{0:T(128)} %param.31) | copy-start | bytes 1540
  140.3 1.2 copy-start
Sparse Core Ops, SparseCore 0:
  104.2 28.9 all-gather.1
where the time goes:
time: 180 us; the launch traced here: 179 us
  Pallas kernels  112 us (62%)
  local copies, waits for them, and re-layouts  17 us (9%)
  between operations  14.5 us (8%)
  waiting for transfers between devices  14.4 us (8%)
  starting transfers between devices  14.1 us (8%)
  other arithmetic  5.28 us (3%)
  matrix products  1.83 us (1%)
    pallas_call x1, Pallas kernels, gather_project(): pl.pallas_call(functools.partial(gather_kernel, cols, sizes, ring), out_s...  59 us
    pallas_call x1, Pallas kernels, project_out(): pl.pallas_call(functools.partial(project_kernel, cols, sizes), out_shape=...  29.4 us
    pallas_call x1, Pallas kernels, delta_terms(): pl.pallas_call(delta_kernel, grid=(units // group,), out_shape=(jax.Shape...  17.1 us
    ppermute x4, waiting for transfers between devices, from_behind(): return lax.ppermute(block, axis, route)  14.3 us
    ppermute x4, starting transfers between devices, from_behind(): return lax.ppermute(block, axis, route)  14.1 us
    unnamed x28, local copies, waits for them, and re-layouts  6.84 us
    pallas_call x1, Pallas kernels, sum_small(): pl.pallas_call(functools.partial(sum_kernel, cols, sizes), out_shape=jax....  6.01 us
  transfers between devices with their start and end apart: 5, of which 2 were waited for; matrix products, arithmetic and copies ran while one was open for 8% of the time, Pallas kernels for 13%

commit v1 on v0

v1 whole, which is shorter than its diff:
```python
import functools

import jax
import jax.numpy as jnp
from jax import lax
from jax.experimental import pallas as pl
from jax.experimental.pallas import tpu as pltpu
from jax.sharding import PartitionSpec as P

HEAD = 128
CHUNK = 128
EPS = 1e-06
HIGH = lax.Precision.HIGHEST
MESH = pl.DeviceIdType.MESH
F32 = jnp.float32
BF16 = jnp.bfloat16


def dot(a, b, dims, precision=None):
    return lax.dot_general(a, b, (dims, ((), ())), preferred_element_type=F32, precision=precision)


def mm(a, b, precision=None):
    return dot(a, b, ((1,), (0,)), precision)


def mm_nt(a, b, precision=None):
    return dot(a, b, ((1,), (1,)), precision)


def mm_tn(a, b, precision=None):
    return dot(a, b, ((0,), (0,)), precision)


def split(x):
    high = x.astype(BF16)
    return high, (x - high.astype(F32)).astype(BF16)


def mm3(a, b, form=mm):
    a_high, a_low = split(a)
    b_high, b_low = split(b)
    return form(a_high, b_high) + (form(a_high, b_low) + form(a_low, b_high))


def mm1(a, b, form=mm):
    return form(a.astype(BF16), b.astype(BF16))


def silu(x):
    return x * jax.nn.sigmoid(x)


def unit(x):
    return x * lax.rsqrt(jnp.sum(x * x, axis=-1, keepdims=True) + EPS)


def softplus(x):
    return jnp.maximum(x, 0.0) + jnp.log1p(jnp.exp(-jnp.abs(x)))


def aligned(index, size):
    return pl.ds(pl.multiple_of(index * size, size), size)


def layer_kernel(
    sizes,
    tok_ref, wq_ref, wk_ref, wv_ref, wu_ref, wg_ref, wd_ref, wc_ref,
    spike_ref, state_ref, gates_ref, gain_ref, rate_ref, bias_ref, head_gain_ref, taps_ref, chan_gain_ref,
    out_ref,
    tok_all, normed, w_all, wo_all, raw, spikes, small, rows_ref, cols_ref,
    t_all, k_all, gamma_all, p_all, u_all, m_all, o_all, p_out, u_out, x_end,
    st_first, st_send, st_recv, ext, tail, rim, conv_ref, stat_ref, sums, mix,
    to_pair, from_pair, to_z, from_z, own_sum,
    z_send, z_recv, x_send, x_recv, y_send, y_recv, a_send, a_recv, b_send, b_recv,
    tok_sem_s, tok_sem_r, misc_s, misc_r, sum_s, sum_r, pair_s, pair_r, zo_s, zo_r, local_sem,
):
    across, ring, down = sizes
    rows, half = tok_ref.shape
    depth, wide_tp = wq_ref.shape
    wide = wide_tp // 2
    heads = wide // HEAD
    pos = 2 * rows
    chunks = pos // CHUNK
    shard = wd_ref.shape[1]
    lines = down * across
    piece = depth // lines
    out_piece = wide // lines
    tap_count = taps_ref.shape[0]
    channels = taps_ref.shape[1]
    pad = ext.shape[0] - pos

    g, s, f, t = (lax.axis_index(name) for name in ("grp", "sp", "fs", "tp"))
    b = lax.rem(s, 2)
    line = g * across + f
    z_at = lambda j: {"sp": lax.rem(s + j, ring)}
    x_at = lambda a: {"fs": lax.rem(f + a, across)}
    y_at = lambda c: {"grp": lax.rem(g + c, down)}
    partner = {"tp": 1 - t}
    z_peer = {"sp": s + 1 - 2 * b}
    far = {"sp": s + 1 - 2 * b, "tp": 1 - t}
    ahead = {"sp": lax.rem(s + 2, ring)}
    z_span, x_span, y_span = range(1, ring), range(1, across), range(1, down)

    def copy(src, dst, send_sem, recv_sem, peer):
        return pltpu.make_async_remote_copy(
            src_ref=src, dst_ref=dst, send_sem=send_sem, recv_sem=recv_sem, device_id=peer, device_id_type=MESH
        )

    weights = (wk_ref, wq_ref, wv_ref, wu_ref, wg_ref)
    out_weights = (wd_ref, wc_ref)
    OUT = len(weights)

    local = [pltpu.make_async_copy(tok_ref, tok_all.at[b, :, aligned(t, half)], local_sem.at[0])]
    local.append(pltpu.make_async_copy(spike_ref, spikes.at[b], local_sem.at[1]))
    for i, w in enumerate(weights):
        local.append(
            pltpu.make_async_copy(w.at[:, aligned(b, wide)], w_all.at[i, aligned(s, depth), :], local_sem.at[2 + i])
        )
    for i, w in enumerate(out_weights):
        local.append(
            pltpu.make_async_copy(w.at[aligned(b, wide), :], wo_all.at[i, :, aligned(s, shard)], local_sem.at[2 + OUT + i])
        )
    for one in local:
        one.start()

    barrier = pltpu.get_barrier_semaphore()
    friends = [z_at(j) for j in z_span] + [x_at(a) for a in x_span] + [y_at(c) for c in y_span] + [partner, far]
    for friend in friends:
        pl.semaphore_signal(barrier, inc=1, device_id=friend, device_id_type=MESH)
    pl.semaphore_wait(barrier, len(friends))

    z_copies = {}

    def z_send_piece(i):
        for j in z_span:
            to = lax.rem(lax.rem(s + j, ring), 2)
            if i < OUT:
                src = weights[i].at[aligned(line, piece), aligned(to, wide)]
                dst = w_all.at[i, pl.ds(pl.multiple_of(s * depth + line * piece, piece), piece), :]
            else:
                begin = pl.multiple_of(to * wide + line * out_piece, out_piece)
                src = out_weights[i - OUT].at[pl.ds(begin, out_piece), :]
                dst = wo_all.at[i - OUT, aligned(line, out_piece), aligned(s, shard)]
            one = copy(src, dst, z_send.at[i, j - 1], z_recv.at[i, j - 1], z_at(j))
            one.start()
            z_copies[i, j] = one

    part = rows // 2
    toks = {}

    def tok_place(side, h, from_tp):
        return tok_all.at[side, pl.ds(h * part, part), aligned(from_tp, half)]

    def tok_z(h):
        toks[h] = copy(
            tok_ref.at[pl.ds(h * part, part), :], tok_place(b, h, t), tok_sem_s.at[h], tok_sem_r.at[h], z_peer
        )
        toks[h].start()

    to_partner = copy(tok_ref, tok_all.at[b, :, aligned(t, half)], tok_sem_s.at[4], tok_sem_r.at[4], partner)
    to_partner.start()
    spike_copy = copy(spike_ref, spikes.at[b], misc_s.at[0], misc_r.at[0], z_peer)
    z_send_piece(0)
    spike_copy.start()
    tok_z(0)
    z_send_piece(1)
    tok_z(1)
    for i in range(2, OUT + len(out_weights)):
        z_send_piece(i)

    def region(i, src, of_line, side=None):
        if i < OUT:
            span = pl.ds(pl.multiple_of(src * depth + of_line * piece, piece), piece)
            lanes = slice(None) if side is None else pl.ds(side * (wide // 2), wide // 2)
            return w_all.at[i, span, lanes]
        which = slice(None) if side is None else pl.ds(side, 1)
        return wo_all.at[which, aligned(of_line, out_piece), aligned(src, shard)]

    x_copies, y_copies, a_copies, b_copies = {}, {}, {}, {}

    def source(j):
        return lax.rem(s + ring - j, ring)

    def first_stage(i):
        for j in z_span:
            for k in [i] if i < OUT else [OUT, OUT + 1]:
                z_copies[k, j].wait_recv()
            block = region(i, source(j), line)
            for a in x_span:
                x_copies[i, j, a] = copy(block, block, x_send.at[i, j - 1, a - 1], x_recv.at[i, j - 1, a - 1], x_at(a))
                x_copies[i, j, a].start()
            for c in y_span:
                y_copies[i, j, c] = copy(block, block, y_send.at[i, j - 1, c - 1], y_recv.at[i, j - 1, c - 1], y_at(c))
                y_copies[i, j, c].start()

    def second_stage(i):
        for j in z_span:
            for a in x_span:
                x_copies[i, j, a].wait_recv()
                behind = g * across + lax.rem(f + across - a, across)
                block = region(i, source(j), behind, 0)
                for c in y_span:
                    one = copy(block, block, a_send.at[i, j - 1, a - 1, c - 1], a_recv.at[i, j - 1, a - 1, c - 1], y_at(c))
                    one.start()
                    a_copies[i, j, a, c] = one
            for c in y_span:
                y_copies[i, j, c].wait_recv()
                behind = lax.rem(g + down - c, down) * across + f
                block = region(i, source(j), behind, 1)
                for a in x_span:
                    one = copy(block, block, b_send.at[i, j - 1, a - 1, c - 1], b_recv.at[i, j - 1, a - 1, c - 1], x_at(a))
                    one.start()
                    b_copies[i, j, a, c] = one

    def drain(i):
        for j in z_span:
            for a in x_span:
                for c in y_span:
                    a_copies[i, j, a, c].wait_recv()
                    b_copies[i, j, a, c].wait_recv()
        if i < OUT:
            local[2 + i].wait()

    def normalise(side):
        step = 32

        @pl.loop(0, rows // step)
        def _(r):
            block = tok_all[side, aligned(r, step), :].astype(F32)
            scale = lax.rsqrt(jnp.mean(block * block, axis=-1, keepdims=True) + EPS)
            span = pl.ds(pl.multiple_of(side * rows + r * step, step), step)
            normed[span, :] = (block * scale * gain_ref[...]).astype(BF16)

        gates = mm(normed[aligned(side, rows), :], gates_ref[...]).astype(BF16).astype(F32)
        small[:, aligned(side, rows)] = gates.T[: small.shape[0]]

    def project(i):
        @pl.loop(0, 2)
        def _(r):
            span = aligned(r, rows)
            raw[i, span, :] = mm(normed[span, :], w_all[i]).astype(BF16)

    row_id = lax.broadcasted_iota(jnp.int32, (CHUNK, CHUNK), 0)
    col_id = lax.broadcasted_iota(jnp.int32, (CHUNK, CHUNK), 1)
    lower = row_id >= col_id
    strict = row_id > col_id
    eye = jnp.where(row_id == col_id, 1.0, 0.0)

    def decays():
        rows_ref[...] = jnp.zeros_like(rows_ref)
        for h in range(heads):
            head = (2 * t + b) * heads + h
            spike = jnp.concatenate([spikes[side, pl.ds(b * heads + h, 1), :] for side in range(2)], axis=1)
            rate = jnp.exp(jnp.full((1, pos), rate_ref[head], F32))
            rows_ref[h : h + 1, :] = -rate * softplus(small[pl.ds(head, 1), :]) + spike
            level = small[pl.ds(small.shape[0] // 2 + head, 1), :] + bias_ref[head]
            rows_ref[heads + h : heads + h + 1, :] = jax.nn.sigmoid(level)
        upper = jnp.where(row_id <= col_id, 1.0, 0.0)
        decay_row = lax.broadcasted_iota(jnp.int32, (rows_ref.shape[0], CHUNK), 0) < heads
        for c in range(chunks):
            lanes = slice(c * CHUNK, (c + 1) * CHUNK)
            block = rows_ref[:, lanes]
            block = jnp.where(decay_row, mm(block, upper, HIGH), block)
            rows_ref[:, lanes] = block
            cols_ref[lanes, :] = jnp.concatenate([block, jnp.zeros((HEAD - block.shape[0], CHUNK), F32)], axis=0).T

    def unit_of(u):
        return u % heads, slice((u // heads) * CHUNK, (u // heads + 1) * CHUNK)

    def lanes_of(h):
        return slice(h * HEAD, (h + 1) * HEAD)

    def cum_col(u):
        h, span = unit_of(u)
        return cols_ref[span, h : h + 1]

    def beta_col(u):
        h, span = unit_of(u)
        return cols_ref[span, heads + h : heads + h + 1]

    def inverses(units):
        a = []
        for u in units:
            h, span = unit_of(u)
            keys = unit(silu(raw[0, span, lanes_of(h)].astype(F32)))
            diff = cum_col(u) - rows_ref[h : h + 1, span]
            gamma = jnp.where(lower, jnp.exp(jnp.where(lower, diff, 0.0)), 0.0)
            k_all[u] = keys
            gamma_all[u] = gamma
            a.append(jnp.where(strict, mm3(keys * beta_col(u), keys, mm_nt) * gamma, 0.0))
        size = 1
        inv = None
        while size < CHUNK:
            pair = 2 * size
            off = (row_id // pair == col_id // pair) & (row_id % pair >= size) & (col_id % pair < size)
            cross = [jnp.where(off, x, 0.0) for x in a]
            if inv is None:
                inv = [eye - x for x in cross]
            else:
                mid = [mm3(x, y) for x, y in zip(cross, inv)]
                inv = [y - mm3(y, x) for x, y in zip(mid, inv)]
            size = pair
        for u, x in zip(units, inv):
            t_all[u] = x

    def blocks(units):
        for u in units:
            h, span = unit_of(u)
            keys = k_all[u]
            query = unit(silu(raw[1, span, lanes_of(h)].astype(F32))) * HEAD ** (-0.5)
            values = silu(raw[2, span, lanes_of(h)].astype(F32))
            cum = cum_col(u)
            beta = beta_col(u)
            grow = jnp.exp(cum)
            last = cum[CHUNK - 1 :, :]
            right = jnp.concatenate([values * beta, keys * beta * grow], axis=1)
            solved = mm3(t_all[u], right)
            q_k = mm1(query, keys, mm_nt) * gamma_all[u]
            inner = mm1(q_k, solved)
            p_all[u] = query * grow - inner[:, HEAD:]
            u_all[u] = inner[:, :HEAD]
            state = mm3(keys * jnp.exp(last - cum), solved, mm_tn)
            m_all[u] = eye * jnp.exp(last) - state[:, HEAD:]
            o_all[u] = state[:, :HEAD]

    def recurrence():
        for h in range(heads):
            p_out[h, :CHUNK, :] = p_all[h]
            u_out[h, :CHUNK, :] = u_all[h]
        x = [jnp.concatenate([o_all[h], m_all[h]], axis=1) for h in range(heads)]
        for c in range(1, chunks):
            span = slice(c * CHUNK, (c + 1) * CHUNK)
            for h in range(heads):
                u = c * heads + h
                out = mm1(p_all[u], x[h])
                u_out[h, span, :] = out[:, :HEAD] + u_all[u]
                p_out[h, span, :] = out[:, HEAD:]
                nxt = mm3(m_all[u], x[h])
                x[h] = jnp.concatenate([nxt[:, :HEAD] + o_all[u], nxt[:, HEAD:]], axis=1)
        for h in range(heads):
            x_end[h] = x[h]

    state_copy = copy(st_send, st_recv, misc_s.at[1], misc_r.at[1], ahead)

    def send_state():
        @pl.when(s + 2 < ring)
        def _():
            for h in range(heads):
                st_send[h] = (x_end[h, :, :HEAD] + mm3(x_end[h, :, HEAD:], st_first[h])).astype(BF16)
            state_copy.start()

    rim_copy = copy(tail, rim, misc_s.at[2], misc_r.at[2], ahead)

    def gated():
        @pl.loop(0, pos // CHUNK)
        def _(r):
            span = aligned(r, CHUNK)
            glu = raw[3, span, :].astype(F32) * jax.nn.sigmoid(raw[4, span, :].astype(F32))
            ext[pl.ds(pl.multiple_of(pad + r * CHUNK, pad), CHUNK), :] = glu.astype(BF16).astype(F32)

        @pl.when(s + 2 < ring)
        def _():
            tail[...] = ext[pos:, :].astype(BF16)
            rim_copy.start()

    my_chan = pl.ds(pl.multiple_of((2 * t + b) * wide, wide), wide)
    step = 64
    lane = lax.broadcasted_iota(jnp.int32, (step, HEAD), 1)

    def convolve(r):
        acc = jnp.zeros((step, wide), F32)
        window = ext[pl.ds(pl.multiple_of(r * step, step), step + pad), :]
        first = pad - tap_count + 1
        for phase in range(8):
            offsets = [o for o in range(first, first + tap_count) if o % 8 == phase]
            shifted = window[phase : offsets[-1] + step]
            for o in offsets:
                tap = taps_ref[o - first : o - first + 1, my_chan]
                acc = acc + tap * shifted[o - phase : o - phase + step]
        conv_ref[aligned(r, step), :] = acc
        total = jnp.sum(acc, axis=-1, keepdims=True)
        squares = jnp.sum(acc * acc, axis=-1, keepdims=True)
        stat_ref[aligned(r, step), :] = jnp.where(lane == 0, total, jnp.where(lane == 1, squares, 0.0))

    local[0].wait()
    to_partner.wait_recv()
    normalise(b)
    first_stage(0)
    forwards = []

    def forward_tok(h):
        toks[h].wait_recv()
        block = tok_place(1 - b, h, t)
        one = copy(block, block, tok_sem_s.at[2 + h], tok_sem_r.at[2 + h], partner)
        one.start()
        forwards.append(one)

    forward_tok(0)
    first_stage(1)
    second_stage(0)
    forward_tok(1)
    first_stage(2)
    second_stage(1)
    for one in forwards:
        one.wait_recv()
    local[1].wait()
    spike_copy.wait_recv()
    normalise(1 - b)
    decays()
    drain(0)
    project(0)
    units = list(range(chunks * heads))
    group = 2 * heads
    inverses(units[:group])
    first_stage(3)
    second_stage(2)
    inverses(units[group:])
    drain(1)
    project(1)
    first_stage(4)
    second_stage(3)
    drain(2)
    project(2)
    blocks(units)
    second_stage(4)
    first_stage(OUT)
    recurrence()

    @pl.when(s < 2)
    def _():
        for h in range(heads):
            st_first[h] = state_ref[b * heads + h]
        send_state()

    drain(3)
    project(3)
    drain(4)
    project(4)
    second_stage(OUT)
    gated()

    @pl.loop(1, pos // step)
    def _(r):
        convolve(r)

    @pl.when(s < 2)
    def _():
        ext[:pad, :] = jnp.zeros((pad, wide), F32)

    @pl.when(s >= 2)
    def _():
        rim_copy.wait_recv()
        ext[:pad, :] = rim[...].astype(F32)

    convolve(0)
    sums[0] = stat_ref[...].T[: sums.shape[1]]
    sum_copies = [
        copy(sums.at[0], sums.at[1 + d], sum_s.at[d], sum_r.at[d], peer)
        for d, peer in enumerate((partner, z_peer, far))
    ]
    for one in sum_copies:
        one.start()

    @pl.when(s >= 2)
    def _():
        state_copy.wait_recv()
        for h in range(heads):
            st_first[h] = st_recv[h].astype(F32)
        send_state()

    for h in range(heads):
        attn = mm1(p_out[h], st_first[h]) + u_out[h]
        attn = attn * lax.rsqrt(jnp.mean(attn * attn, axis=-1, keepdims=True) + EPS) * head_gain_ref[...]
        mix[:, lanes_of(h)] = attn.astype(BF16)

    for one in sum_copies:
        one.wait_recv()
    total = sums[0] + sums[1] + sums[2] + sums[3]
    mean = total[0:1] / channels
    scale = lax.rsqrt(total[1:2] / channels - mean * mean + EPS)
    stats = jnp.concatenate([mean, scale, jnp.zeros((HEAD - 2, pos), F32)], axis=0)
    stat_ref[...] = stats.T

    @pl.loop(0, pos // step)
    def _(r):
        span = aligned(r, step)
        stat = stat_ref[span, :]
        value = (conv_ref[span, :] - stat[:, 0:1]) * stat[:, 1:2] * chan_gain_ref[:, my_chan]
        mix[span, wide:] = silu(value).astype(BF16)

    drain(OUT)
    for one in local[2 + OUT :]:
        one.wait()
    width = to_z.shape[2]
    parts = half // width

    def product(side, c, of_tp):
        block = mix[aligned(side, rows), :]
        lanes = pl.ds(pl.multiple_of(of_tp * half + c * width, width), width)
        return mm(block[:, :wide], wo_all[0, :, lanes]) + mm(block[:, wide:], wo_all[1, :, lanes])

    order = [(p, c) for p in range(2) for c in range(parts)]
    pairs, z_outs = {}, {}

    def give(p, c):
        to_pair[p, c] = product(1 - b if p == 0 else b, c, 1 - t).astype(BF16)
        one = copy(to_pair.at[p, c], from_pair.at[p, c], pair_s.at[p, c], pair_r.at[p, c], partner)
        one.start()
        pairs[p, c] = one

    give(*order[0])
    for at, (p, c) in enumerate(order):
        if at + 1 < len(order):
            give(*order[at + 1])
        mine = product(1 - b if p == 0 else b, c, t)
        pairs[p, c].wait_recv()
        mine = mine + from_pair[p, c].astype(F32)
        if p == 0:
            to_z[c] = mine.astype(BF16)
            one = copy(to_z.at[c], from_z.at[c], zo_s.at[c], zo_r.at[c], z_peer)
            one.start()
            z_outs[c] = one
        else:
            own_sum[c] = mine
    for c in range(parts):
        z_outs[c].wait_recv()
        out_ref[:, c * width : (c + 1) * width] = (own_sum[c] + from_z[c].astype(F32)).astype(BF16)

    for group_of in (z_copies, x_copies, y_copies, a_copies, b_copies, toks, pairs, z_outs):
        for one in group_of.values():
            one.wait_send()
    for one in [to_partner, spike_copy] + forwards + sum_copies:
        one.wait_send()

    @pl.when(s + 2 < ring)
    def _():
        state_copy.wait_send()
        rim_copy.wait_send()


def layer(sizes, tokens, weights, outs, spikes, states, gates, gain, rate, bias, head_gain, taps, chan_gain):
    across, ring, down = sizes
    rows, half = tokens.shape
    depth, wide_tp = weights[0].shape
    wide = wide_tp // 2
    heads = wide // HEAD
    pos = 2 * rows
    chunks = pos // CHUNK
    units = chunks * heads
    total = 2 * half
    pad = -(-(taps.shape[0] - 1) // 32) * 32
    width = min(256, half)
    parts = half // width
    dma = pltpu.SemaphoreType.DMA
    vmem = pl.BlockSpec(memory_space=pltpu.VMEM)
    smem = pl.BlockSpec(memory_space=pltpu.SMEM)
    anywhere = pl.BlockSpec(memory_space=pl.ANY)
    scratch = pltpu.VMEM
    square = (units, CHUNK, HEAD)
    pieces, spread = 7, 6
    hops, x_hops, y_hops = (max(size - 1, 1) for size in (ring, across, down))
    return pl.pallas_call(
        functools.partial(layer_kernel, sizes),
        out_shape=jax.ShapeDtypeStruct((rows, half), BF16),
        in_specs=[anywhere] * 8 + [vmem] * 4 + [smem] * 2 + [vmem] * 3,
        out_specs=vmem,
        scratch_shapes=[
            scratch((2, rows, total), BF16),
            scratch((pos, total), BF16),
            scratch((5, depth * ring, wide), BF16),
            scratch((2, wide, total), BF16),
            scratch((5, pos, wide), BF16),
            scratch((2,) + spikes.shape, F32),
            scratch((gates.shape[1] // 8, pos), F32),
            scratch((8, pos), F32),
            scratch((pos, HEAD), F32),
            scratch((units, CHUNK, CHUNK), F32),
            scratch(square, F32),
            scratch((units, CHUNK, CHUNK), F32),
            scratch(square, F32),
            scratch(square, F32),
            scratch((units, HEAD, HEAD), F32),
            scratch((units, HEAD, HEAD), F32),
            scratch((heads, pos, HEAD), F32),
            scratch((heads, pos, HEAD), F32),
            scratch((heads, HEAD, 2 * HEAD), F32),
            scratch((heads, HEAD, HEAD), F32),
            scratch((heads, HEAD, HEAD), BF16),
            scratch((heads, HEAD, HEAD), BF16),
            scratch((pad + pos, wide), F32),
            scratch((pad, wide), BF16),
            scratch((pad, wide), BF16),
            scratch((pos, wide), F32),
            scratch((pos, HEAD), F32),
            scratch((4, 8, pos), F32),
            scratch((pos, 2 * wide), BF16),
            scratch((2, parts, rows, width), BF16),
            scratch((2, parts, rows, width), BF16),
            scratch((parts, rows, width), BF16),
            scratch((parts, rows, width), BF16),
            scratch((parts, rows, width), F32),
            dma((pieces, hops)), dma((pieces, hops)),
            dma((spread, hops, x_hops)), dma((spread, hops, x_hops)),
            dma((spread, hops, y_hops)), dma((spread, hops, y_hops)),
            dma((spread, hops, x_hops, y_hops)), dma((spread, hops, x_hops, y_hops)),
            dma((spread, hops, x_hops, y_hops)), dma((spread, hops, x_hops, y_hops)),
            dma((5,)), dma((5,)), dma((3,)), dma((3,)), dma((3,)), dma((3,)),
            dma((2, parts)), dma((2, parts)), dma((parts,)), dma((parts,)),
            dma((9,)),
        ],
        compiler_params=pltpu.CompilerParams(
            collective_id=1, has_side_effects=True, vmem_limit_bytes=56 * 1024 * 1024
        ),
        name="layer",
    )(tokens, *weights, *outs, spikes, states, gates, gain, rate, bias, head_gain, taps, chan_gain)


def on_device(
    tokens,
    input_norm_gain,
    query_weight,
    key_weight,
    value_weight,
    decay_gate_weight,
    write_strength_weight,
    up_weight,
    gate_half_weight,
    log_decay_rate,
    write_strength_bias,
    decay_spike_added,
    starting_state,
    head_norm_gain,
    convolution_kernel,
    channel_norm_gain,
    delta_output_rows,
    convolution_output_rows,
):
    sizes = (lax.axis_size("fs"), lax.axis_size("sp"), lax.axis_size("grp"))
    heads_tp = decay_spike_added.shape[2]
    heads = decay_gate_weight.shape[1]
    gates = jnp.concatenate([decay_gate_weight, write_strength_weight], axis=1)
    gates = jnp.pad(gates, ((0, 0), (0, 128 - 2 * heads)))
    spikes = jnp.pad(decay_spike_added[0].T, ((0, -heads_tp % 8), (0, 0)))
    return layer(
        sizes,
        tokens[0],
        (query_weight, key_weight, value_weight, up_weight, gate_half_weight),
        (delta_output_rows, convolution_output_rows),
        spikes,
        starting_state[0],
        gates,
        input_norm_gain[None],
        log_decay_rate,
        write_strength_bias,
        head_norm_gain[None],
        convolution_kernel,
        channel_norm_gain[None],
    )[None]


def solution(mesh):
    return jax.shard_map(
        on_device,
        mesh=mesh,
        in_specs=(
            P(("grp", "fs"), "sp", "tp"),
            P(),
            P("sp", "tp"),
            P("sp", "tp"),
            P("sp", "tp"),
            P(),
            P(),
            P("sp", "tp"),
            P("sp", "tp"),
            P(),
            P(),
            P(("grp", "fs"), "sp", "tp"),
            P(("grp", "fs"), "tp", None, None),
            P(),
            P(),
            P(),
            P("tp", "sp"),
            P("tp", "sp"),
        ),
        out_specs=P(("grp", "fs"), "sp", "tp"),
        check_vma=False,
    )
```

time: 180 us -> 103 us (0.57)
  between operations: 14.5 us -> 0.02 us
  Pallas kernels: 112 us -> 97.6 us
  waiting for transfers between devices: 14.4 us -> 0 us
  starting transfers between devices: 14.1 us -> 0 us
  local copies, waits for them, and re-layouts: 17 us -> 4.32 us
  other arithmetic: 5.28 us -> 0.78 us
  matrix products: 1.83 us -> 0 us
    ppermute x4 -> x0, waiting for transfers between devices: 14.3 us -> none  [from_behind(): return lax.ppermute(block, axis, route)]
    ppermute x4 -> x0, starting transfers between devices: 14.1 us -> none  [from_behind(): return lax.ppermute(block, axis, route)]
    pallas_call x4 -> x1, Pallas kernels: 112 us -> 97.6 us  [layer(): pl.pallas_call(functools.partial(layer_kernel, sizes), out_shape=jax.Shap...]
    unnamed x28 -> x3, local copies, waits for them, and re-layouts: 6.84 us -> 2.56 us
    dynamic_slice x6 -> x0, local copies, waits for them, and re-layouts: 3.84 us -> none  [the longest x1 0.99 us: mine(): return lax.dynamic_slice_in_dim(weight, col * width, width, axis)]
    reduce_sum x1 -> x0, other arithmetic: 2.4 us -> none  [on_device(): sums = jnp.stack([jnp.sum(conv, axis=-1), jnp.sum(conv * conv, axis=-1)])]
    mul x2 -> x0, local copies, waits for them, and re-layouts: 2.27 us -> none  [on_device(): conv = conv + taps_here[tap] * extended[:, tap:tap + rows]]
    dot_general x5 -> x0, matrix products: 1.83 us -> none  [the longest x3 1.18 us: on_device(): sent = jnp.einsum('hde,hef->hdf', maps, state, precision=HIGH) + offsets]
  transfers between devices with their start and end apart: 5 -> 0, of which waited for: 2 -> 0; matrix products, arithmetic and copies ran while one was open for 8% -> 0% of each run, Pallas kernels for 13% -> 0%
where the time goes in v1:
time: 103 us
  Pallas kernels  97.6 us (95%)
  local copies, waits for them, and re-layouts  4.32 us (4%)
    pallas_call x1, Pallas kernels, layer(): pl.pallas_call(functools.partial(layer_kernel, sizes), out_shape=jax.Shap...  97.6 us
    unnamed x3, local copies, waits for them, and re-layouts  2.56 us

profile of v1, /device:TPU:0, one launch (start us, length us, event | category | flops | bytes accessed | tf_op | source)
XLA Modules:
  0.0 102.7 jit_solution(17317271648143709324)
XLA Ops:
  0.0 0.0 copy-start
  0.0 0.7 copy-done
  0.7 0.6 pad.8.spike_ref
  1.3 0.8 pad_maximum_fusion
  2.1 0.3 copy.21
  2.3 0.9 pad.9.gates_ref
  3.2 97.6 %layer.1 = bf16[256,1024]{1,0:T(8,128)(2,1)} custom-call(bf16[256,1024]{1,0:T(8,128)(2,1)} %bitcast.10, bf16[512,512]{1,0:T(8,128)(2,1)} %wq_ref.1, bf16[512,512]{1,0:T(8,128)(2,1)} %wk_ref.1, bf16[512,512]{1,0:T(8,128)(2,1)} %wv_ref.1, bf16[512,512]{1,0:T(8,128)(2,1)} %wu_ref.1, bf16[512,512]{1,0:T(8,128)(2,1)} %wg_ref.1, bf16[512,512]{1,0:T(8,128)(2,1)} %wd_ref.1, ...), custom_call_target="tpu_custom_call" | custom-call | tf_op jit(solution)/shard_map/layer/pallas_call | solution.py:563
  100.8 1.9 %copy.23 = bf16[1,256,1024]{2,1,0:T(8,128)(2,1)} copy(bf16[1,256,1024]{2,1,0:T(8,128)(2,1)} %bitcast.9) | data formatting | bytes 1048576
Async XLA Ops:
  0.0 0.7 copy-start

commit v2 on v1

--- a/solution.py
+++ b/solution.py
@@ -59,6 +59,11 @@
     return jnp.maximum(x, 0.0) + jnp.log1p(jnp.exp(-jnp.abs(x)))
 
 
+def row_of(block, row):
+    here = lax.broadcasted_iota(jnp.int32, block.shape, 0) == row
+    return jnp.sum(jnp.where(here, block, 0.0), axis=0, keepdims=True)
+
+
 def aligned(index, size):
     return pl.ds(pl.multiple_of(index * size, size), size)
 
@@ -66,7 +71,7 @@
 def layer_kernel(
     sizes,
     tok_ref, wq_ref, wk_ref, wv_ref, wu_ref, wg_ref, wd_ref, wc_ref,
-    spike_ref, state_ref, gates_ref, gain_ref, rate_ref, bias_ref, head_gain_ref, taps_ref, chan_gain_ref,
+    spike_ref, state_ref, decay_ref, write_ref, gain_ref, rate_ref, bias_ref, head_gain_ref, taps_ref, chan_gain_ref,
     out_ref,
     tok_all, normed, w_all, wo_all, raw, spikes, small, rows_ref, cols_ref,
     t_all, k_all, gamma_all, p_all, u_all, m_all, o_all, p_out, u_out, x_end,
@@ -112,14 +117,14 @@
     OUT = len(weights)
 
     local = [pltpu.make_async_copy(tok_ref, tok_all.at[b, :, aligned(t, half)], local_sem.at[0])]
-    local.append(pltpu.make_async_copy(spike_ref, spikes.at[b], local_sem.at[1]))
+    local.append(pltpu.make_async_copy(spike_ref, spikes.at[b], local_sem.at[1 + OUT + len(out_weights)]))
     for i, w in enumerate(weights):
         local.append(
-            pltpu.make_async_copy(w.at[:, aligned(b, wide)], w_all.at[i, aligned(s, depth), :], local_sem.at[2 + i])
+            pltpu.make_async_copy(w.at[:, aligned(b, wide)], w_all.at[i, aligned(s, depth), :], local_sem.at[1 + i])
         )
     for i, w in enumerate(out_weights):
         local.append(
-            pltpu.make_async_copy(w.at[aligned(b, wide), :], wo_all.at[i, :, aligned(s, shard)], local_sem.at[2 + OUT + i])
+            pltpu.make_async_copy(w.at[aligned(b, wide), :], wo_all.at[i, :, aligned(s, shard)], local_sem.at[1 + OUT + i])
         )
     for one in local:
         one.start()
@@ -161,21 +166,23 @@
     to_partner = copy(tok_ref, tok_all.at[b, :, aligned(t, half)], tok_sem_s.at[4], tok_sem_r.at[4], partner)
     to_partner.start()
     spike_copy = copy(spike_ref, spikes.at[b], misc_s.at[0], misc_r.at[0], z_peer)
-    z_send_piece(0)
     spike_copy.start()
+    for i in range(OUT - 1):
+        z_send_piece(i)
     tok_z(0)
-    z_send_piece(1)
+    z_send_piece(OUT - 1)
+    z_send_piece(OUT)
     tok_z(1)
-    for i in range(2, OUT + len(out_weights)):
-        z_send_piece(i)
+    z_send_piece(OUT + 1)
 
     def region(i, src, of_line, side=None):
         if i < OUT:
             span = pl.ds(pl.multiple_of(src * depth + of_line * piece, piece), piece)
             lanes = slice(None) if side is None else pl.ds(side * (wide // 2), wide // 2)
             return w_all.at[i, span, lanes]
-        which = slice(None) if side is None else pl.ds(side, 1)
-        return wo_all.at[which, aligned(of_line, out_piece), aligned(src, shard)]
+        count = out_piece if side is None else out_piece // 2
+        begin = of_line * out_piece + (0 if side is None else side * count)
+        return wo_all.at[i - OUT, pl.ds(pl.multiple_of(begin, count), count), aligned(src, shard)]
 
     x_copies, y_copies, a_copies, b_copies = {}, {}, {}, {}
 
@@ -184,8 +191,7 @@
 
     def first_stage(i):
         for j in z_span:
-            for k in [i] if i < OUT else [OUT, OUT + 1]:
-                z_copies[k, j].wait_recv()
+            z_copies[i, j].wait_recv()
             block = region(i, source(j), line)
             for a in x_span:
                 x_copies[i, j, a] = copy(block, block, x_send.at[i, j - 1, a - 1], x_recv.at[i, j - 1, a - 1], x_at(a))
@@ -213,33 +219,36 @@
                     one.start()
                     b_copies[i, j, a, c] = one
 
-    def drain(i):
-        for j in z_span:
+    def drain(i, hops=z_span):
+        for j in hops:
             for a in x_span:
                 for c in y_span:
                     a_copies[i, j, a, c].wait_recv()
                     b_copies[i, j, a, c].wait_recv()
-        if i < OUT:
+        if hops is z_span:
             local[2 + i].wait()
 
-    def normalise(side):
+    def rows_at(start, count):
+        return pl.ds(pl.multiple_of(start, CHUNK), count)
+
+    def normalise(side, begin, count):
         step = 32
 
-        @pl.loop(0, rows // step)
+        @pl.loop(0, count // step)
         def _(r):
-            block = tok_all[side, aligned(r, step), :].astype(F32)
+            block = tok_all[side, pl.ds(pl.multiple_of(begin + r * step, step), step), :].astype(F32)
             scale = lax.rsqrt(jnp.mean(block * block, axis=-1, keepdims=True) + EPS)
-            span = pl.ds(pl.multiple_of(side * rows + r * step, step), step)
+            span = pl.ds(pl.multiple_of(side * rows + begin + r * step, step), step)
             normed[span, :] = (block * scale * gain_ref[...]).astype(BF16)
 
-        gates = mm(normed[aligned(side, rows), :], gates_ref[...]).astype(BF16).astype(F32)
-        small[:, aligned(side, rows)] = gates.T[: small.shape[0]]
-
-    def project(i):
-        @pl.loop(0, 2)
-        def _(r):
-            span = aligned(r, rows)
-            raw[i, span, :] = mm(normed[span, :], w_all[i]).astype(BF16)
+        span = rows_at(side * rows + begin, count)
+        block = normed[span, :]
+        for w, gate_ref in enumerate((decay_ref, write_ref)):
+            small[w, :, span] = mm_nt(gate_ref[...], block).astype(BF16).astype(F32)
+
+    def project(i, start, count):
+        span = rows_at(start, count)
+        raw[i, span, :] = mm(normed[span, :], w_all[i]).astype(BF16)
 
     row_id = lax.broadcasted_iota(jnp.int32, (CHUNK, CHUNK), 0)
     col_id = lax.broadcasted_iota(jnp.int32, (CHUNK, CHUNK), 1)
@@ -247,26 +256,35 @@
     strict = row_id > col_id
     eye = jnp.where(row_id == col_id, 1.0, 0.0)
 
-    def decays():
-        rows_ref[...] = jnp.zeros_like(rows_ref)
+    rows_ref[...] = jnp.zeros_like(rows_ref)
+
+    def decays(side, begin, count):
+        span = rows_at(side * rows + begin, count)
         for h in range(heads):
             head = (2 * t + b) * heads + h
-            spike = jnp.concatenate([spikes[side, pl.ds(b * heads + h, 1), :] for side in range(2)], axis=1)
-            rate = jnp.exp(jnp.full((1, pos), rate_ref[head], F32))
-            rows_ref[h : h + 1, :] = -rate * softplus(small[pl.ds(head, 1), :]) + spike
-            level = small[pl.ds(small.shape[0] // 2 + head, 1), :] + bias_ref[head]
-            rows_ref[heads + h : heads + h + 1, :] = jax.nn.sigmoid(level)
+            rate = jnp.exp(jnp.full((1, count), rate_ref[head], F32))
+            spike = row_of(spikes[side, :, begin : begin + count], b * heads + h)
+            rows_ref[h : h + 1, span] = -rate * softplus(row_of(small[0, :, span], head)) + spike
+            level = row_of(small[1, :, span], head) + bias_ref[head]
+            rows_ref[heads + h : heads + h + 1, span] = jax.nn.sigmoid(level)
         upper = jnp.where(row_id <= col_id, 1.0, 0.0)
         decay_row = lax.broadcasted_iota(jnp.int32, (rows_ref.shape[0], CHUNK), 0) < heads
-        for c in range(chunks):
-            lanes = slice(c * CHUNK, (c + 1) * CHUNK)
+        for c in range(count // CHUNK):
+            lanes = rows_at(side * rows + begin + c * CHUNK, CHUNK)
             block = rows_ref[:, lanes]
             block = jnp.where(decay_row, mm(block, upper, HIGH), block)
             rows_ref[:, lanes] = block
             cols_ref[lanes, :] = jnp.concatenate([block, jnp.zeros((HEAD - block.shape[0], CHUNK), F32)], axis=0).T
 
+    def units_of(start, count):
+        first = start // CHUNK
+        return [(h, first + c) for c in range(count // CHUNK) for h in range(heads)]
+
     def unit_of(u):
-        return u % heads, slice((u // heads) * CHUNK, (u // heads + 1) * CHUNK)
+        return u[0], aligned(u[1], CHUNK)
+
+    def slot(u):
+        return u[1] * heads + u[0]
 
     def lanes_of(h):
         return slice(h * HEAD, (h + 1) * HEAD)
@@ -279,15 +297,16 @@
         h, span = unit_of(u)
         return cols_ref[span, heads + h : heads + h + 1]
 
-    def inverses(units):
+    def inverses(start, count):
+        units = units_of(start, count)
         a = []
         for u in units:
             h, span = unit_of(u)
             keys = unit(silu(raw[0, span, lanes_of(h)].astype(F32)))
             diff = cum_col(u) - rows_ref[h : h + 1, span]
             gamma = jnp.where(lower, jnp.exp(jnp.where(lower, diff, 0.0)), 0.0)
-            k_all[u] = keys
-            gamma_all[u] = gamma
+            k_all[slot(u)] = keys
+            gamma_all[slot(u)] = gamma
             a.append(jnp.where(strict, mm3(keys * beta_col(u), keys, mm_nt) * gamma, 0.0))
         size = 1
         inv = None
@@ -302,12 +321,12 @@
                 inv = [y - mm3(y, x) for x, y in zip(mid, inv)]
             size = pair
         for u, x in zip(units, inv):
-            t_all[u] = x
-
-    def blocks(units):
-        for u in units:
+            t_all[slot(u)] = x
+
+    def blocks(start, count):
+        for u in units_of(start, count):
             h, span = unit_of(u)
-            keys = k_all[u]
+            keys = k_all[slot(u)]
             query = unit(silu(raw[1, span, lanes_of(h)].astype(F32))) * HEAD ** (-0.5)
             values = silu(raw[2, span, lanes_of(h)].astype(F32))
             cum = cum_col(u)
@@ -315,14 +334,14 @@
             grow = jnp.exp(cum)
             last = cum[CHUNK - 1 :, :]
             right = jnp.concatenate([values * beta, keys * beta * grow], axis=1)
-            solved = mm3(t_all[u], right)
-            q_k = mm1(query, keys, mm_nt) * gamma_all[u]
+            solved = mm3(t_all[slot(u)], right)
+            q_k = mm1(query, keys, mm_nt) * gamma_all[slot(u)]
             inner = mm1(q_k, solved)
-            p_all[u] = query * grow - inner[:, HEAD:]
-            u_all[u] = inner[:, :HEAD]
+            p_all[slot(u)] = query * grow - inner[:, HEAD:]
+            u_all[slot(u)] = inner[:, :HEAD]
             state = mm3(keys * jnp.exp(last - cum), solved, mm_tn)
-            m_all[u] = eye * jnp.exp(last) - state[:, HEAD:]
-            o_all[u] = state[:, :HEAD]
+            m_all[slot(u)] = eye * jnp.exp(last) - state[:, HEAD:]
+            o_all[slot(u)] = state[:, :HEAD]
 
     def recurrence():
         for h in range(heads):
@@ -383,10 +402,9 @@
         squares = jnp.sum(acc * acc, axis=-1, keepdims=True)
         stat_ref[aligned(r, step), :] = jnp.where(lane == 0, total, jnp.where(lane == 1, squares, 0.0))
 
-    local[0].wait()
-    to_partner.wait_recv()
-    normalise(b)
-    first_stage(0)
+    mine = b * rows
+    peers = (1 - b) * rows
+    peers_late = peers + part
     forwards = []
 
     def forward_tok(h):
@@ -396,35 +414,56 @@
         one.start()
         forwards.append(one)
 
-    forward_tok(0)
+    local[0].wait()
+    local[1].wait()
+    to_partner.wait_recv()
+    normalise(b, 0, rows)
+    decays(b, 0, rows)
+    first_stage(0)
     first_stage(1)
     second_stage(0)
-    forward_tok(1)
     first_stage(2)
     second_stage(1)
-    for one in forwards:
-        one.wait_recv()
-    local[1].wait()
+    first_stage(3)
+    drain(0)
+    project(0, mine, rows)
+    inverses(mine, rows)
+    second_stage(2)
+    forward_tok(0)
+    drain(1)
+    project(1, mine, rows)
     spike_copy.wait_recv()
-    normalise(1 - b)
-    decays()
-    drain(0)
-    project(0)
-    units = list(range(chunks * heads))
-    group = 2 * heads
-    inverses(units[:group])
-    first_stage(3)
-    second_stage(2)
-    inverses(units[group:])
-    drain(1)
-    project(1)
+    forwards[0].wait_recv()
+    normalise(1 - b, 0, part)
+    decays(1 - b, 0, part)
     first_stage(4)
     second_stage(3)
     drain(2)
-    project(2)
-    blocks(units)
+    project(2, mine, rows)
+    blocks(mine, rows)
+    first_stage(OUT)
+    for i in range(3):
+        project(i, peers, part)
+    inverses(peers, part)
     second_stage(4)
-    first_stage(OUT)
+    drain(3)
+    project(3, mine, rows)
+    project(3, peers, part)
+    forward_tok(1)
+    blocks(peers, part)
+    forwards[1].wait_recv()
+    normalise(1 - b, part, part)
+    decays(1 - b, part, part)
+    second_stage(OUT)
+    for i in range(4):
+        project(i, peers_late, part)
+    drain(4)
+    project(4, mine, rows)
+    project(4, peers, rows)
+    first_stage(OUT + 1)
+    gated()
+    inverses(peers_late, part)
+    blocks(peers_late, part)
     recurrence()
 
     @pl.when(s < 2)
@@ -433,16 +472,11 @@
             st_first[h] = state_ref[b * heads + h]
         send_state()
 
-    drain(3)
-    project(3)
-    drain(4)
-    project(4)
-    second_stage(OUT)
-    gated()
-
     @pl.loop(1, pos // step)
     def _(r):
         convolve(r)
+
+    second_stage(OUT + 1)
 
     @pl.when(s < 2)
     def _():
@@ -489,45 +523,56 @@
         value = (conv_ref[span, :] - stat[:, 0:1]) * stat[:, 1:2] * chan_gain_ref[:, my_chan]
         mix[span, wide:] = silu(value).astype(BF16)
 
-    drain(OUT)
     for one in local[2 + OUT :]:
         one.wait()
+    turns = ring // 2
     width = to_z.shape[2]
-    parts = half // width
-
-    def product(side, c, of_tp):
+    parts = shard // width
+
+    def product(side, lane, of_tp):
         block = mix[aligned(side, rows), :]
-        lanes = pl.ds(pl.multiple_of(of_tp * half + c * width, width), width)
+        lanes = pl.ds(pl.multiple_of(of_tp * half + lane, width), width)
         return mm(block[:, :wide], wo_all[0, :, lanes]) + mm(block[:, wide:], wo_all[1, :, lanes])
 
-    order = [(p, c) for p in range(2) for c in range(parts)]
-    pairs, z_outs = {}, {}
-
-    def give(p, c):
-        to_pair[p, c] = product(1 - b if p == 0 else b, c, 1 - t).astype(BF16)
-        one = copy(to_pair.at[p, c], from_pair.at[p, c], pair_s.at[p, c], pair_r.at[p, c], partner)
+    order = [(k, p, c) for k in range(turns) for p in range(2) for c in range(parts)]
+    pairs = {}
+
+    def place(k, c):
+        return lax.rem(lax.rem(s, turns) + k, turns) * parts + c
+
+    def give(k, p, c):
+        if p == 0 and c == 0:
+            for j in ((turns - k) % turns, (turns - k) % turns + turns):
+                if j:
+                    drain(OUT, (j,))
+                    drain(OUT + 1, (j,))
+        at = k * parts + c
+        to_pair[p, at] = product(1 - b if p == 0 else b, place(k, c) * width, 1 - t).astype(BF16)
+        one = copy(to_pair.at[p, at], from_pair.at[p, at], pair_s.at[p, at], pair_r.at[p, at], partner)
         one.start()
-        pairs[p, c] = one
+        pairs[k, p, c] = one
+
+    def slot_copy(at):
+        return copy(to_z.at[at], from_z.at[at], zo_s.at[at], zo_r.at[at], z_peer)
 
     give(*order[0])
-    for at, (p, c) in enumerate(order):
+    for at, (k, p, c) in enumerate(order):
         if at + 1 < len(order):
             give(*order[at + 1])
-        mine = product(1 - b if p == 0 else b, c, t)
-        pairs[p, c].wait_recv()
-        mine = mine + from_pair[p, c].astype(F32)
+        mine = product(1 - b if p == 0 else b, place(k, c) * width, t)
+        pairs[k, p, c].wait_recv()
+        mine = mine + from_pair[p, k * parts + c].astype(F32)
         if p == 0:
-            to_z[c] = mine.astype(BF16)
-            one = copy(to_z.at[c], from_z.at[c], zo_s.at[c], zo_r.at[c], z_peer)
-            one.start()
-            z_outs[c] = one
+            to_z[place(k, c)] = mine.astype(BF16)
+            slot_copy(place(k, c)).start()
         else:
-            own_sum[c] = mine
-    for c in range(parts):
-        z_outs[c].wait_recv()
-        out_ref[:, c * width : (c + 1) * width] = (own_sum[c] + from_z[c].astype(F32)).astype(BF16)
-
-    for group_of in (z_copies, x_copies, y_copies, a_copies, b_copies, toks, pairs, z_outs):
+            own_sum[place(k, c)] = mine
+    for at in range(turns * parts):
+        slot_copy(at).wait_recv()
+        out_ref[:, at * width : (at + 1) * width] = (own_sum[at] + from_z[at].astype(F32)).astype(BF16)
+        slot_copy(at).wait_send()
+
+    for group_of in (z_copies, x_copies, y_copies, a_copies, b_copies, toks, pairs):
         for one in group_of.values():
             one.wait_send()
     for one in [to_partner, spike_copy] + forwards + sum_copies:
@@ -539,7 +584,7 @@
         rim_copy.wait_send()
 
 
-def layer(sizes, tokens, weights, outs, spikes, states, gates, gain, rate, bias, head_gain, taps, chan_gain):
+def layer(sizes, tokens, weights, outs, spikes, states, decay_gates, write_gates, gain, rate, bias, head_gain, taps, chan_gain):
     across, ring, down = sizes
     rows, half = tokens.shape
     depth, wide_tp = weights[0].shape
@@ -550,7 +595,7 @@
     units = chunks * heads
     total = 2 * half
     pad = -(-(taps.shape[0] - 1) // 32) * 32
-    width = min(256, half)
+    width = min(256, outs[0].shape[1])
     parts = half // width
     dma = pltpu.SemaphoreType.DMA
     vmem = pl.BlockSpec(memory_space=pltpu.VMEM)
@@ -558,12 +603,12 @@
     anywhere = pl.BlockSpec(memory_space=pl.ANY)
     scratch = pltpu.VMEM
     square = (units, CHUNK, HEAD)
-    pieces, spread = 7, 6
+    pieces = spread = 7
     hops, x_hops, y_hops = (max(size - 1, 1) for size in (ring, across, down))
     return pl.pallas_call(
         functools.partial(layer_kernel, sizes),
         out_shape=jax.ShapeDtypeStruct((rows, half), BF16),
-        in_specs=[anywhere] * 8 + [vmem] * 4 + [smem] * 2 + [vmem] * 3,
+        in_specs=[anywhere] * 8 + [vmem] * 5 + [smem] * 2 + [vmem] * 3,
         out_specs=vmem,
         scratch_shapes=[
             scratch((2, rows, total), BF16),
@@ -572,7 +617,7 @@
             scratch((2, wide, total), BF16),
             scratch((5, pos, wide), BF16),
             scratch((2,) + spikes.shape, F32),
-            scratch((gates.shape[1] // 8, pos), F32),
+            scratch((2, decay_gates.shape[0], pos), F32),
             scratch((8, pos), F32),
             scratch((pos, HEAD), F32),
             scratch((units, CHUNK, CHUNK), F32),
@@ -613,7 +658,7 @@
             collective_id=1, has_side_effects=True, vmem_limit_bytes=56 * 1024 * 1024
         ),
         name="layer",
-    )(tokens, *weights, *outs, spikes, states, gates, gain, rate, bias, head_gain, taps, chan_gain)
+    )(tokens, *weights, *outs, spikes, states, decay_gates, write_gates, gain, rate, bias, head_gain, taps, chan_gain)
 
 
 def on_device(
@@ -637,19 +682,15 @@
     convolution_output_rows,
 ):
     sizes = (lax.axis_size("fs"), lax.axis_size("sp"), lax.axis_size("grp"))
-    heads_tp = decay_spike_added.shape[2]
-    heads = decay_gate_weight.shape[1]
-    gates = jnp.concatenate([decay_gate_weight, write_strength_weight], axis=1)
-    gates = jnp.pad(gates, ((0, 0), (0, 128 - 2 * heads)))
-    spikes = jnp.pad(decay_spike_added[0].T, ((0, -heads_tp % 8), (0, 0)))
     return layer(
         sizes,
         tokens[0],
         (query_weight, key_weight, value_weight, up_weight, gate_half_weight),
         (delta_output_rows, convolution_output_rows),
-        spikes,
+        decay_spike_added[0].T,
         starting_state[0],
-        gates,
+        decay_gate_weight.T,
+        write_strength_weight.T,
         input_norm_gain[None],
         log_decay_rate,
         write_strength_bias,

time: 103 us -> 88.1 us (0.86)
  Pallas kernels: 97.6 us -> 86 us
  local copies, waits for them, and re-layouts: 4.32 us -> 1.87 us
    pallas_call x1, Pallas kernels: 97.6 us -> 86 us  [layer(): pl.pallas_call(functools.partial(layer_kernel, sizes), out_shape=jax.Shap...]
    pad x2 -> x0, local copies, waits for them, and re-layouts: 1.5 us -> none  [the longest x1 0.9 us: on_device(): gates = jnp.pad(gates, ((0, 0), (0, 128 - 2 * heads)))]
    unnamed x3 -> x1, local copies, waits for them, and re-layouts: 2.56 us -> 1.87 us
where the time goes in v2:
time: 88.1 us; the launch traced here: 87.9 us
  Pallas kernels  86 us (98%)
  local copies, waits for them, and re-layouts  1.87 us (2%)
    pallas_call x1, Pallas kernels, layer(): pl.pallas_call(functools.partial(layer_kernel, sizes), out_shape=jax.Shap...  86 us
    unnamed x1, local copies, waits for them, and re-layouts  1.87 us

profile of v2, /device:TPU:0, one launch (start us, length us, event | category | flops | bytes accessed | tf_op | source)
XLA Modules:
  0.0 87.9 jit_solution(6368823893521364646)
XLA Ops:
  0.0 86.0 %layer.1 = bf16[256,1024]{1,0:T(8,128)(2,1)} custom-call(bf16[256,1024]{1,0:T(8,128)(2,1)} %bitcast.12, bf16[512,512]{1,0:T(8,128)(2,1)} %wq_ref.1, bf16[512,512]{1,0:T(8,128)(2,1)} %wk_ref.1, bf16[512,512]{1,0:T(8,128)(2,1)} %wv_ref.1, bf16[512,512]{1,0:T(8,128)(2,1)} %wu_ref.1, bf16[512,512]{1,0:T(8,128)(2,1)} %wg_ref.1, bf16[512,512]{1,0:T(8,128)(2,1)} %wd_ref.1, ...), custom_call_target="tpu_custom_call" | custom-call | tf_op jit(solution)/shard_map/layer/pallas_call | solution.py:608
  86.0 1.9 %copy.20 = bf16[1,256,1024]{2,1,0:T(8,128)(2,1)} copy(bf16[1,256,1024]{2,1,0:T(8,128)(2,1)} %bitcast.11) | data formatting | bytes 1048576

commit v3 on v2

--- a/solution.py
+++ b/solution.py
@@ -115,6 +115,13 @@
     weights = (wk_ref, wq_ref, wv_ref, wu_ref, wg_ref)
     out_weights = (wd_ref, wc_ref)
     OUT = len(weights)
+    width = to_z.shape[2]
+    splits = shard // width
+    turns = half // shard
+
+    def out_lanes(i, src):
+        return pl.ds(pl.multiple_of(src * shard + (i - OUT) * width, width), width)
+
 
     local = [pltpu.make_async_copy(tok_ref, tok_all.at[b, :, aligned(t, half)], local_sem.at[0])]
     local.append(pltpu.make_async_copy(spike_ref, spikes.at[b], local_sem.at[1 + OUT + len(out_weights)]))
@@ -143,13 +150,17 @@
             if i < OUT:
                 src = weights[i].at[aligned(line, piece), aligned(to, wide)]
                 dst = w_all.at[i, pl.ds(pl.multiple_of(s * depth + line * piece, piece), piece), :]
+                z_copies[i, j] = [copy(src, dst, z_send.at[i, j - 1], z_recv.at[i, j - 1], z_at(j))]
             else:
                 begin = pl.multiple_of(to * wide + line * out_piece, out_piece)
-                src = out_weights[i - OUT].at[pl.ds(begin, out_piece), :]
-                dst = wo_all.at[i - OUT, aligned(line, out_piece), aligned(s, shard)]
-            one = copy(src, dst, z_send.at[i, j - 1], z_recv.at[i, j - 1], z_at(j))
-            one.start()
-            z_copies[i, j] = one
+                z_copies[i, j] = []
+                for half_of, w in enumerate(out_weights):
+                    src = w.at[pl.ds(begin, out_piece), pl.ds((i - OUT) * width, width)]
+                    dst = wo_all.at[half_of, aligned(line, out_piece), out_lanes(i, s)]
+                    at = OUT + 2 * (i - OUT) + half_of
+                    z_copies[i, j].append(copy(src, dst, z_send.at[at, j - 1], z_recv.at[at, j - 1], z_at(j)))
+            for one in z_copies[i, j]:
+                one.start()
 
     part = rows // 2
     toks = {}
@@ -171,18 +182,20 @@
         z_send_piece(i)
     tok_z(0)
     z_send_piece(OUT - 1)
-    z_send_piece(OUT)
     tok_z(1)
-    z_send_piece(OUT + 1)
+    for i in range(OUT, OUT + splits):
+        z_send_piece(i)
 
     def region(i, src, of_line, side=None):
         if i < OUT:
-            span = pl.ds(pl.multiple_of(src * depth + of_line * piece, piece), piece)
+            begin = src * depth + of_line * piece
+            if side is not None and piece % 32 == 0:
+                count = piece // 2
+                return w_all.at[i, pl.ds(pl.multiple_of(begin + side * count, count), count), :]
             lanes = slice(None) if side is None else pl.ds(side * (wide // 2), wide // 2)
-            return w_all.at[i, span, lanes]
-        count = out_piece if side is None else out_piece // 2
-        begin = of_line * out_piece + (0 if side is None else side * count)
-        return wo_all.at[i - OUT, pl.ds(pl.multiple_of(begin, count), count), aligned(src, shard)]
+            return w_all.at[i, pl.ds(pl.multiple_of(begin, piece), piece), lanes]
+        which = slice(None) if side is None else pl.ds(side, 1)
+        return wo_all.at[which, aligned(of_line, out_piece), out_lanes(i, src)]
 
     x_copies, y_copies, a_copies, b_copies = {}, {}, {}, {}
 
@@ -191,7 +204,8 @@
 
     def first_stage(i):
         for j in z_span:
-            z_copies[i, j].wait_recv()
+            for one in z_copies[i, j]:
+                one.wait_recv()
             block = region(i, source(j), line)
             for a in x_span:
                 x_copies[i, j, a] = copy(block, block, x_send.at[i, j - 1, a - 1], x_recv.at[i, j - 1, a - 1], x_at(a))
@@ -219,13 +233,13 @@
                     one.start()
                     b_copies[i, j, a, c] = one
 
-    def drain(i, hops=z_span):
-        for j in hops:
+    def drain(i):
+        for j in z_span:
             for a in x_span:
                 for c in y_span:
                     a_copies[i, j, a, c].wait_recv()
                     b_copies[i, j, a, c].wait_recv()
-        if hops is z_span:
+        if i < OUT:
             local[2 + i].wait()
 
     def rows_at(start, count):
@@ -441,28 +455,28 @@
     drain(2)
     project(2, mine, rows)
     blocks(mine, rows)
-    first_stage(OUT)
     for i in range(3):
         project(i, peers, part)
     inverses(peers, part)
+    forward_tok(1)
     second_stage(4)
-    drain(3)
-    project(3, mine, rows)
-    project(3, peers, part)
-    forward_tok(1)
     blocks(peers, part)
     forwards[1].wait_recv()
     normalise(1 - b, part, part)
     decays(1 - b, part, part)
-    second_stage(OUT)
-    for i in range(4):
+    for i in range(3):
         project(i, peers_late, part)
+    first_stage(OUT)
+    inverses(peers_late, part)
+    drain(3)
+    project(3, mine, rows)
+    project(3, peers, rows)
     drain(4)
     project(4, mine, rows)
     project(4, peers, rows)
-    first_stage(OUT + 1)
     gated()
-    inverses(peers_late, part)
+    for i in range(OUT + 1, OUT + splits):
+        first_stage(i)
     blocks(peers_late, part)
     recurrence()
 
@@ -476,7 +490,7 @@
     def _(r):
         convolve(r)
 
-    second_stage(OUT + 1)
+    second_stage(OUT)
 
     @pl.when(s < 2)
     def _():
@@ -523,56 +537,53 @@
         value = (conv_ref[span, :] - stat[:, 0:1]) * stat[:, 1:2] * chan_gain_ref[:, my_chan]
         mix[span, wide:] = silu(value).astype(BF16)
 
+    for i in range(OUT + 1, OUT + splits):
+        second_stage(i)
     for one in local[2 + OUT :]:
         one.wait()
-    turns = ring // 2
-    width = to_z.shape[2]
-    parts = shard // width
-
-    def product(side, lane, of_tp):
+
+    def product(side, at, of_tp):
         block = mix[aligned(side, rows), :]
-        lanes = pl.ds(pl.multiple_of(of_tp * half + lane, width), width)
+        lanes = pl.ds(pl.multiple_of(of_tp * half + at * width, width), width)
         return mm(block[:, :wide], wo_all[0, :, lanes]) + mm(block[:, wide:], wo_all[1, :, lanes])
 
-    order = [(k, p, c) for k in range(turns) for p in range(2) for c in range(parts)]
-    pairs = {}
-
-    def place(k, c):
-        return lax.rem(lax.rem(s, turns) + k, turns) * parts + c
-
-    def give(k, p, c):
-        if p == 0 and c == 0:
-            for j in ((turns - k) % turns, (turns - k) % turns + turns):
-                if j:
-                    drain(OUT, (j,))
-                    drain(OUT + 1, (j,))
-        at = k * parts + c
-        to_pair[p, at] = product(1 - b if p == 0 else b, place(k, c) * width, 1 - t).astype(BF16)
-        one = copy(to_pair.at[p, at], from_pair.at[p, at], pair_s.at[p, at], pair_r.at[p, at], partner)
-        one.start()
-        pairs[k, p, c] = one
-
-    def slot_copy(at):
-        return copy(to_z.at[at], from_z.at[at], zo_s.at[at], zo_r.at[at], z_peer)
+    order = [(k, p, m) for k in range(splits) for p in range(2) for m in range(turns)]
+    pairs, z_outs = {}, {}
+
+    def give(k, p, m):
+        if p == 0 and m == 0:
+            drain(OUT + k)
+        at = m * splits + k
+        to_pair[p, at] = product(1 - b if p == 0 else b, at, 1 - t).astype(BF16)
+        pairs[p, at] = copy(to_pair.at[p, at], from_pair.at[p, at], pair_s.at[p, at], pair_r.at[p, at], partner)
+        pairs[p, at].start()
+
+    def finish(at):
+        z_outs[at].wait_recv()
+        out_ref[:, at * width : (at + 1) * width] = (own_sum[at] + from_z[at].astype(F32)).astype(BF16)
 
     give(*order[0])
-    for at, (k, p, c) in enumerate(order):
-        if at + 1 < len(order):
-            give(*order[at + 1])
-        mine = product(1 - b if p == 0 else b, place(k, c) * width, t)
-        pairs[k, p, c].wait_recv()
-        mine = mine + from_pair[p, k * parts + c].astype(F32)
+    for n, (k, p, m) in enumerate(order):
+        if n + 1 < len(order):
+            give(*order[n + 1])
+        at = m * splits + k
+        value = product(1 - b if p == 0 else b, at, t)
+        pairs[p, at].wait_recv()
+        value = value + from_pair[p, at].astype(F32)
         if p == 0:
-            to_z[place(k, c)] = mine.astype(BF16)
-            slot_copy(place(k, c)).start()
+            to_z[at] = value.astype(BF16)
+            z_outs[at] = copy(to_z.at[at], from_z.at[at], zo_s.at[at], zo_r.at[at], z_peer)
+            z_outs[at].start()
         else:
-            own_sum[place(k, c)] = mine
-    for at in range(turns * parts):
-        slot_copy(at).wait_recv()
-        out_ref[:, at * width : (at + 1) * width] = (own_sum[at] + from_z[at].astype(F32)).astype(BF16)
-        slot_copy(at).wait_send()
-
-    for group_of in (z_copies, x_copies, y_copies, a_copies, b_copies, toks, pairs):
+            own_sum[at] = value
+    for k in range(splits):
+        for m in range(turns):
+            finish(m * splits + k)
+
+    for ones in z_copies.values():
+        for one in ones:
+            one.wait_send()
+    for group_of in (x_copies, y_copies, a_copies, b_copies, toks, pairs, z_outs):
         for one in group_of.values():
             one.wait_send()
     for one in [to_partner, spike_copy] + forwards + sum_copies:
@@ -603,7 +614,8 @@
     anywhere = pl.BlockSpec(memory_space=pl.ANY)
     scratch = pltpu.VMEM
     square = (units, CHUNK, HEAD)
-    pieces = spread = 7
+    splits = outs[0].shape[1] // width
+    pieces, spread = 5 + 2 * splits, 5 + splits
     hops, x_hops, y_hops = (max(size - 1, 1) for size in (ring, across, down))
     return pl.pallas_call(
         functools.partial(layer_kernel, sizes),

time: 88.1 us -> 85.5 us (0.970)
  Pallas kernels: 86 us -> 83.5 us
    pallas_call x1, Pallas kernels: 86 us -> 83.5 us  [layer(): pl.pallas_call(functools.partial(layer_kernel, sizes), out_shape=jax.Shap...]
where the time goes in v3:
time: 85.5 us; the launch traced here: 85.3 us
  Pallas kernels  83.5 us (98%)
  local copies, waits for them, and re-layouts  1.87 us (2%)
    pallas_call x1, Pallas kernels, layer(): pl.pallas_call(functools.partial(layer_kernel, sizes), out_shape=jax.Shap...  83.5 us
    unnamed x1, local copies, waits for them, and re-layouts  1.87 us

profile of v3, /device:TPU:0, one launch (start us, length us, event | category | flops | bytes accessed | tf_op | source)
XLA Modules:
  0.0 85.3 jit_solution(2321134517980523406)
XLA Ops:
  0.0 83.5 %layer.1 = bf16[256,1024]{1,0:T(8,128)(2,1)} custom-call(bf16[256,1024]{1,0:T(8,128)(2,1)} %bitcast.12, bf16[512,512]{1,0:T(8,128)(2,1)} %wq_ref.1, bf16[512,512]{1,0:T(8,128)(2,1)} %wk_ref.1, bf16[512,512]{1,0:T(8,128)(2,1)} %wv_ref.1, bf16[512,512]{1,0:T(8,128)(2,1)} %wu_ref.1, bf16[512,512]{1,0:T(8,128)(2,1)} %wg_ref.1, bf16[512,512]{1,0:T(8,128)(2,1)} %wd_ref.1, ...), custom_call_target="tpu_custom_call" | custom-call | tf_op jit(solution)/shard_map/layer/pallas_call | solution.py:620
  83.5 1.9 %copy.20 = bf16[1,256,1024]{2,1,0:T(8,128)(2,1)} copy(bf16[1,256,1024]{2,1,0:T(8,128)(2,1)} %bitcast.11) | data formatting | bytes 1048576
